TPU v7x, 32 devices: a whole 2x2x4 slice. The times are simulated.
32 devices in a mesh: sp: 16 (over z, y, core), tp: 2 (over x).
Axes of the slice: x: 2, y: 2, z: 4, core: 2. Of those that a mesh axis runs over, the one named last changes fastest.
Arguments:
- query_rows: bfloat16 [8192, 1024], P(('sp', 'tp')), may hold values from -6 to 6
- key_rows: bfloat16 [8192, 1024], P(('sp', 'tp')), may hold values from -6 to 6
- value_rows: bfloat16 [8192, 1024], P(('sp', 'tp')), may hold values from -6 to 6
- out_grad: bfloat16 [8192, 1024], P(('sp', 'tp')), may hold values from -40 to 40
- log_totals: float32 [8192, 8], P(('sp', 'tp')), may hold values from 6 to 7.5
- out_dot: float32 [8192, 8], P(('sp', 'tp')), may hold values from -6 to 6
- bias_table: float32 [8, 320], replicated, may hold values from -4 to 4
Outputs:
- grad_query: bfloat16 [8192, 1024], P(('sp', 'tp'))
- grad_key: bfloat16 [8192, 1024], P(('sp', 'tp'))
- grad_value: bfloat16 [8192, 1024], P(('sp', 'tp'))
- grad_table: float32 [8, 320], replicated
All inputs are finite; a program needn't handle non-finite values.
Results may differ from a plain program's by a relative error of at most 0.005.
Values may be sent and summed in bfloat16 or wider, within the bound.
No kernel may reach another device: no remote copies, remote signals or barrier semaphores. Data moves between devices by JAX's collectives and lax.ppermute only.
A program may use at most 128 MiB of HBM per device.

v0:
```python
import jax
import jax.numpy as jnp
from jax import lax
from jax.sharding import PartitionSpec as P

SEG_LEN = 64
LEFT_SEGS = 8
REL_CLIP = 256


def passed_along(block, axis, distance):
    devices = range(lax.axis_size(axis))
    route = [(i - distance, i) for i in devices if i - distance in devices]
    return lax.ppermute(block, axis, route)


def band_matrix(diagonal_vals, row_count, col_count):
    head_count = diagonal_vals.shape[0]
    span_width = row_count + col_count - 1
    repeated = jnp.broadcast_to(diagonal_vals[:, None, :], (head_count, row_count, span_width))
    flat_rows = jnp.pad(
        repeated.reshape(head_count, row_count * span_width), ((0, 0), (0, row_count))
    )
    shaped = flat_rows.reshape(head_count, row_count, span_width + 1)[:, :, :col_count]
    return shaped[:, :, ::-1]


def diagonal_sums(matrix_vals):
    head_count, row_count, col_count = matrix_vals.shape
    span_width = row_count + col_count - 1
    flipped = jnp.pad(matrix_vals[:, :, ::-1], ((0, 0), (0, 0), (0, row_count)))
    skewed = flipped.reshape(head_count, row_count * (col_count + row_count))[
        :, : row_count * span_width
    ]
    return jnp.sum(skewed.reshape(head_count, row_count, span_width), axis=1)


def table_onehot(offset, row_count, col_count, table_len):
    diagonals = jnp.arange(row_count + col_count - 1, dtype=jnp.int32)
    distance = jnp.clip(offset + diagonals - (col_count - 1), 1 - SEG_LEN, REL_CLIP) + SEG_LEN - 1
    return (distance[:, None] == jnp.arange(table_len, dtype=jnp.int32)[None, :]).astype(
        jnp.float32
    )


def bias_block(bias_table, offset, row_count, col_count):
    onehot_map = table_onehot(offset, row_count, col_count, bias_table.shape[1])
    diagonal_vals = jnp.dot(bias_table, onehot_map.T, precision=lax.Precision.HIGHEST)
    return (band_matrix(diagonal_vals, row_count, col_count), onehot_map)


def band_stack(rows, block_count, span_segs):
    segmented = rows.reshape(-1, SEG_LEN, rows.shape[1])
    pieces = [segmented[start : start + block_count] for start in range(span_segs)]
    return jnp.stack(pieces, axis=1).reshape(block_count, span_segs * SEG_LEN, rows.shape[1])


def band_terms(queries, grads_out, log_rows, dot_rows, keys, values, bias_vals, allowed):
    block_count, query_count, feature_count = queries.shape
    key_count = keys.shape[1]
    head_count = log_rows.shape[2]
    query_heads = queries.reshape(block_count, query_count, head_count, -1)
    grad_heads = grads_out.reshape(block_count, query_count, head_count, -1)
    key_heads = keys.reshape(block_count, key_count, head_count, -1)
    value_heads = values.reshape(block_count, key_count, head_count, -1)
    inv_root = query_heads.shape[3] ** (-0.5)
    raw_scores = jnp.einsum(
        "bqhd,bkhd->bhqk", query_heads, key_heads, preferred_element_type=jnp.float32
    )
    scores = raw_scores * inv_root + bias_vals[None]
    log_terms = jnp.transpose(log_rows, (0, 2, 1))[:, :, :, None]
    dot_terms = jnp.transpose(dot_rows, (0, 2, 1))[:, :, :, None]
    weights = jnp.exp(scores - log_terms)
    weights = jnp.where(allowed[:, None, None, :], weights, 0.0)
    weight_grads = jnp.einsum(
        "bqhd,bkhd->bhqk", grad_heads, value_heads, preferred_element_type=jnp.float32
    )
    score_grads = weights * (weight_grads - dot_terms)
    return (
        weights.astype(jnp.bfloat16),
        score_grads.astype(jnp.bfloat16),
        score_grads,
        query_heads,
        key_heads,
        grad_heads,
        inv_root,
    )


def local(query_rows, key_rows, value_rows, out_grad, log_totals, out_dot, bias_table):
    row_count = query_rows.shape[0]
    feature_count = query_rows.shape[1]
    head_count = log_totals.shape[1]
    seg_count = row_count // SEG_LEN
    span_segs = LEFT_SEGS + 1
    band_len = span_segs * SEG_LEN
    need_rows = LEFT_SEGS * SEG_LEN
    lag_total = -(-need_rows // row_count)
    skip_rows = lag_total * row_count - need_rows
    first_row = lax.axis_index(("sp", "tp")) * row_count
    earlier = []
    for lag_count in range(lag_total, 0, -1):
        start_row = skip_rows if lag_count == lag_total else 0
        earlier.append(passed_along((key_rows, value_rows), ("sp", "tp"), lag_count))
    all_keys = jnp.concatenate([pair[0] for pair in earlier] + [key_rows], axis=0)
    all_values = jnp.concatenate([pair[1] for pair in earlier] + [value_rows], axis=0)
    key_bands = band_stack(all_keys, seg_count, span_segs)
    value_bands = band_stack(all_values, seg_count, span_segs)
    band_pos = (
        jnp.arange(seg_count, dtype=jnp.int32)[:, None] * SEG_LEN
        + jnp.arange(band_len, dtype=jnp.int32)[None, :]
    )
    allowed = first_row - need_rows + band_pos >= 0
    bias_vals, onehot_map = bias_block(bias_table, need_rows, SEG_LEN, band_len)
    weights_b, score_grads_b, score_grads, query_heads, key_heads, grad_heads, inv_root = (
        band_terms(
            query_rows.reshape(seg_count, SEG_LEN, feature_count),
            out_grad.reshape(seg_count, SEG_LEN, feature_count),
            log_totals.reshape(seg_count, SEG_LEN, head_count),
            out_dot.reshape(seg_count, SEG_LEN, head_count),
            key_bands,
            value_bands,
            bias_vals,
            allowed,
        )
    )
    tap_part = jnp.dot(
        diagonal_sums(jnp.sum(score_grads, axis=0)), onehot_map, precision=lax.Precision.HIGHEST
    )
    query_part = jnp.einsum(
        "bhqk,bkhd->bqhd", score_grads_b, key_heads, preferred_element_type=jnp.float32
    )
    grad_query = (query_part * inv_root).reshape(row_count, feature_count).astype(jnp.bfloat16)
    key_band_grad = jnp.einsum(
        "bhqk,bqhd->bkhd", score_grads_b, query_heads, preferred_element_type=jnp.float32
    )
    key_band_grad = (key_band_grad * inv_root).reshape(seg_count, span_segs, SEG_LEN, feature_count)
    value_band_grad = jnp.einsum(
        "bhqk,bqhd->bkhd", weights_b, grad_heads, preferred_element_type=jnp.float32
    )
    value_band_grad = value_band_grad.reshape(seg_count, span_segs, SEG_LEN, feature_count)
    key_all = sum(
        (
            jnp.pad(key_band_grad[:, lag], ((lag, LEFT_SEGS - lag), (0, 0), (0, 0)))
            for lag in range(span_segs)
        )
    ).reshape(-1, feature_count)
    value_all = sum(
        (
            jnp.pad(value_band_grad[:, lag], ((lag, LEFT_SEGS - lag), (0, 0), (0, 0)))
            for lag in range(span_segs)
        )
    ).reshape(-1, feature_count)
    key_total = key_all[need_rows:]
    value_total = value_all[need_rows:]
    for lag_count in range(1, lag_total + 1):
        lower_row = max(need_rows - lag_count * row_count, 0)
        upper_row = need_rows - (lag_count - 1) * row_count
        returned = passed_along(
            (key_all[lower_row:upper_row], value_all[lower_row:upper_row]), ("sp", "tp"), -lag_count
        )
        lead_rows = row_count - (upper_row - lower_row)
        key_total = key_total + returned[0]
        value_total = value_total + returned[1]
    grad_table = lax.psum(tap_part, ("sp", "tp"))
    return (
        grad_query,
        key_total.astype(jnp.bfloat16),
        value_total.astype(jnp.bfloat16),
        grad_table,
    )


def solution(mesh):
    placed = (
        P(("sp", "tp"), None),
        P(("sp", "tp"), None),
        P(("sp", "tp"), None),
        P(("sp", "tp"), None),
        P(("sp", "tp"), None),
        P(("sp", "tp"), None),
        P(),
    )
    return jax.shard_map(
        local,
        mesh=mesh,
        in_specs=placed,
        out_specs=(P(("sp", "tp"), None), P(("sp", "tp"), None), P(("sp", "tp"), None), P()),
        check_vma=False,
    )
```

profile of v0, /device:TPU:0, one launch (start us, length us, event | category | flops | bytes accessed | tf_op | source)
XLA Modules:
  0.0 198.3 jit_solution(5561602564015735739)
XLA Ops:
  0.6 5.7 %collective-permute-start.1 = (bf16[256,1024]{1,0:T(8,128)(2,1)}, bf16[256,1024]{1,0:T(8,128)(2,1)}, u32[]{:S(2)}, u32[]{:S(2)}) collective-permute-start(bf16[256,1024]{1,0:T(8,128)(2,1)} %param.8), channel_id=1, source_target_pairs={{0,1},{1,2},{2,3},{3,4},{4,5},{5,6},{6,7},{7,8},{8,9},{9,10},{10,1... | collective-permute-start | bytes 1572872 | tf_op jit(solution)/shard_map/ppermute | solution.py:14
  6.3 2.1 %collective-permute-start = (bf16[256,1024]{1,0:T(8,128)(2,1)}, bf16[256,1024]{1,0:T(8,128)(2,1)}, u32[]{:S(2)}, u32[]{:S(2)}) collective-permute-start(bf16[256,1024]{1,0:T(8,128)(2,1)} %param.8), channel_id=1, source_target_pairs={{0,2},{1,3},{2,4},{3,5},{4,6},{5,7},{6,8},{7,9},{8,10},{9,11},{10,... | collective-permute-start | bytes 1572872 | tf_op jit(solution)/shard_map/ppermute | solution.py:14
  8.4 4.1 %collective-permute-start.3 = (bf16[256,1024]{1,0:T(8,128)(2,1)}, bf16[256,1024]{1,0:T(8,128)(2,1)}, u32[]{:S(2)}, u32[]{:S(2)}) collective-permute-start(bf16[256,1024]{1,0:T(8,128)(2,1)} %param.9), channel_id=1, source_target_pairs={{0,1},{1,2},{2,3},{3,4},{4,5},{5,6},{6,7},{7,8},{8,9},{9,10},{10,1... | collective-permute-start | bytes 1572872 | tf_op jit(solution)/shard_map/ppermute | solution.py:14
  12.6 2.1 %collective-permute-start.2 = (bf16[256,1024]{1,0:T(8,128)(2,1)}, bf16[256,1024]{1,0:T(8,128)(2,1)}, u32[]{:S(2)}, u32[]{:S(2)}) collective-permute-start(bf16[256,1024]{1,0:T(8,128)(2,1)} %param.9), channel_id=1, source_target_pairs={{0,2},{1,3},{2,4},{3,5},{4,6},{5,7},{6,8},{7,9},{8,10},{9,11},{10,... | collective-permute-start | bytes 1572872 | tf_op jit(solution)/shard_map/ppermute | solution.py:14
  16.9 1.1 copy.172
  18.1 1.9 copy.175
  24.6 3.6 %collective-permute-done.3 = bf16[256,1024]{1,0:T(8,128)(2,1)} collective-permute-done((bf16[256,1024]{1,0:T(8,128)(2,1)}, bf16[256,1024]{1,0:T(8,128)(2,1)}, u32[]{:S(2)}, u32[]{:S(2)}) %collective-permute-start.3) | collective-permute-done | bytes 524320 | tf_op jit(solution)/shard_map/ppermute | solution.py:14
  28.2 1.2 constant_dynamic-update-slice_fusion.16
  30.0 1.2 constant_dynamic-update-slice_fusion.3
  34.1 1.2 copy.174
  37.8 1.2 copy.171
  39.1 1.7 fusion.5
  41.3 5.0 %convolution_bitcast_fusion = f32[4,576,8,128]{3,1,2,0:T(8,128)} fusion(f32[4,8,576,64]{2,3,1,0:T(8,128)S(1)} %fusion.5, f32[4,8,64]{2,1,0:T(8,128)S(1)} %get-tuple-element.49, f32[8,64,576]{2,1,0:T(8,128)S(1)} %slice.268, pred[4,576]{1,0:T(4,128)(4,1)S(1)} %add_compare_fusion, bf16[4,64,8,128]{3,2,1,0:T(8,128)(2,1)S(1)} %bitcast.221), kind=kOutput, calls=%fused_computation.13 | convolution fusion | flops 307888128 | bytes 15870208 | tf_op jit(solution)/shard_map/bhqk,bqhd->bkhd/dot_general | solution.py:138
  46.3 4.2 %fusion.52 = (f32[8,64,576]{2,1,0:T(8,128)S(1)}, bf16[4,8,64,576]{3,2,1,0:T(8,128)(2,1)}) fusion(f32[4,8,64]{2,1,0:T(8,128)S(1)} %get-tuple-element.48, bf16[4,64,8,128]{3,2,1,0:T(8,128)(2,1)S(1)} %bitcast.222, bf16[4,576,8,128]{3,2,1,0:T(8,128)(2,1)S(1)} %bitcast.220, f32[4,8,64]{2,1,0:T(8,128)S(1)} %get-tuple-element.49, f32[8,64,576]{2,1,0:T(8,128)S(1)} %slice.268, ...), kind=kOutput, calls=%fused_computation.101 | convolution fusion | flops 311132160 | bytes 14698752 | tf_op jit(solution)/shard_map/bqhd,bkhd->bhqk/dot_general | solution.py:75
  52.8 1.3 reshape.121
  54.2 12.8 %copy.146 = f32[4,576,8,128]{3,2,1,0:T(8,128)} copy(f32[4,576,8,128]{3,1,2,0:T(8,128)} %convolution_bitcast_fusion) | data formatting | bytes 18874368 | tf_op jit(solution)/shard_map/bhqk,bqhd->bkhd/transpose | solution.py:138
  67.0 11.2 %reshape.119 = f32[4,9,64,1024]{3,2,1,0:T(8,128)} reshape(f32[4,576,8,128]{3,2,1,0:T(8,128)} %copy.146) | data formatting | bytes 18874368 | tf_op jit(solution)/shard_map/reshape | solution.py:141
  78.2 4.7 %slice_bitcast_fusion.8 = (f32[4,64,1024]{2,1,0:T(8,128)S(1)}, f32[4,64,1024]{2,1,0:T(8,128)S(1)}, f32[4,64,1024]{2,1,0:T(8,128)S(1)}, f32[4,64,1024]{2,1,0:T(8,...) fusion(f32[4,9,64,1024]{3,2,1,0:T(8,128)} %reshape.119), kind=kLoop, calls=%fused_computation.37 | loop fusion | bytes 18874368 | tf_op jit(solution)/shard_map/squeeze | solution.py:150
  83.8 1.6 fusion.46
  85.5 1.3 collective-permute-start.7
  86.8 1.5 collective-permute-start.6
  88.3 1.5 multiply_bitcast_fusion
  89.8 9.1 %copy.136 = f32[4,576,8,128]{3,2,1,0:T(8,128)} copy(f32[4,576,8,128]{3,1,2,0:T(8,128)S(1)} %multiply_bitcast_fusion) | data formatting | bytes 18874368 | tf_op jit(solution)/shard_map/mul | solution.py:137
  98.9 11.1 %reshape.118 = f32[4,9,64,1024]{3,2,1,0:T(8,128)} reshape(f32[4,576,8,128]{3,2,1,0:T(8,128)} %copy.136) | data formatting | bytes 18874368 | tf_op jit(solution)/shard_map/reshape | solution.py:137
  110.0 4.7 %slice_bitcast_fusion.17 = (f32[4,64,1024]{2,1,0:T(8,128)S(1)}, f32[4,64,1024]{2,1,0:T(8,128)S(1)}, f32[4,64,1024]{2,1,0:T(8,128)S(1)}, f32[4,64,1024]{2,1,0:T(8...) fusion(f32[4,9,64,1024]{3,2,1,0:T(8,128)} %reshape.118), kind=kLoop, calls=%fused_computation.46 | loop fusion | bytes 18874368 | tf_op jit(solution)/shard_map/squeeze | solution.py:144
  115.8 1.7 fusion.47
  117.5 1.4 collective-permute-start.5
  118.9 1.3 collective-permute-start.4
  120.2 1.2 fusion.28
  123.2 70.2 %psum.7 = f32[8,320]{1,0:T(8,128)} all-reduce(f32[8,320]{1,0:T(8,128)S(1)} %fusion.37), channel_id=1, replica_groups=mesh['sp'=16,'tp'=2] {'sp','tp'}, use_global_device_ids=true, to_apply=%region_2.3 | all-reduce | flops 2560 | bytes 20480 | tf_op jit(solution)/shard_map/psum | solution.py:165
  193.4 2.6 %fusion.34 = bf16[256,1024]{1,0:T(8,128)(2,1)} fusion(f32[256,1024]{1,0:T(8,128)} %collective-permute-done.7, f32[256,1024]{1,0:T(8,128)} %collective-permute-done.6, f32[4,64,1024]{2,1,0:T(8,128)S(1)} %get-tuple-element.22), kind=kLoop, calls=%fused_computation.49 | loop fusion | flops 786432 | bytes 3670016 | tf_op jit(solution)/shard_map/convert_element_type | solution.py:169
  196.0 2.3 %fusion.36 = bf16[256,1024]{1,0:T(8,128)(2,1)} fusion(f32[256,1024]{1,0:T(8,128)S(1)} %collective-permute-done.5, f32[256,1024]{1,0:T(8,128)} %collective-permute-done.4, f32[4,64,1024]{2,1,0:T(8,128)S(1)} %get-tuple-element.25), kind=kLoop, calls=%fused_computation.52 | loop fusion | flops 786432 | bytes 3670016 | tf_op jit(solution)/shard_map/convert_element_type | solution.py:168
  (75 shorter events, 19.1 us)
Async XLA Ops:
  0.6 14.0 %copy-start = (f32[8,320]{1,0:T(8,128)S(1)}, f32[8,320]{1,0:T(8,128)}, u32[]{:S(2)}) copy-start(f32[8,320]{1,0:T(8,128)} %param.13) | copy-start | bytes 30724
  0.6 29.3 %collective-permute-start.1 = (bf16[256,1024]{1,0:T(8,128)(2,1)}, bf16[256,1024]{1,0:T(8,128)(2,1)}, u32[]{:S(2)}, u32[]{:S(2)}) collective-permute-start(bf16[256,1024]{1,0:T(8,128)(2,1)} %param.8), channel_id=1, source_target_pairs={{0,1},{1,2},{2,3},{3,4},{4,5},{5,6},{6,7},{7,8},{8,9},{9,10},{10,1... | collective-permute-start | bytes 1572872 | tf_op jit(solution)/shard_map/ppermute | solution.py:14
  6.3 17.2 %collective-permute-start = (bf16[256,1024]{1,0:T(8,128)(2,1)}, bf16[256,1024]{1,0:T(8,128)(2,1)}, u32[]{:S(2)}, u32[]{:S(2)}) collective-permute-start(bf16[256,1024]{1,0:T(8,128)(2,1)} %param.8), channel_id=1, source_target_pairs={{0,2},{1,3},{2,4},{3,5},{4,6},{5,7},{6,8},{7,9},{8,10},{9,11},{10,... | collective-permute-start | bytes 1572872 | tf_op jit(solution)/shard_map/ppermute | solution.py:14
  8.4 19.8 %collective-permute-start.3 = (bf16[256,1024]{1,0:T(8,128)(2,1)}, bf16[256,1024]{1,0:T(8,128)(2,1)}, u32[]{:S(2)}, u32[]{:S(2)}) collective-permute-start(bf16[256,1024]{1,0:T(8,128)(2,1)} %param.9), channel_id=1, source_target_pairs={{0,1},{1,2},{2,3},{3,4},{4,5},{5,6},{6,7},{7,8},{8,9},{9,10},{10,1... | collective-permute-start | bytes 1572872 | tf_op jit(solution)/shard_map/ppermute | solution.py:14
  12.6 9.9 %collective-permute-start.2 = (bf16[256,1024]{1,0:T(8,128)(2,1)}, bf16[256,1024]{1,0:T(8,128)(2,1)}, u32[]{:S(2)}, u32[]{:S(2)}) collective-permute-start(bf16[256,1024]{1,0:T(8,128)(2,1)} %param.9), channel_id=1, source_target_pairs={{0,2},{1,3},{2,4},{3,5},{4,6},{5,7},{6,8},{7,9},{8,10},{9,11},{10,... | collective-permute-start | bytes 1572872 | tf_op jit(solution)/shard_map/ppermute | solution.py:14
  22.0 7.4 %copy-start.6 = (bf16[256,1024]{1,0:T(8,128)(2,1)S(1)}, bf16[256,1024]{1,0:T(8,128)(2,1)}, u32[]{:S(2)}) copy-start(bf16[256,1024]{1,0:T(8,128)(2,1)} %param.9) | copy-start | bytes 1572868
  29.4 1.7 copy-start.7
  39.0 2.2 %copy-start.2 = (bf16[288,8,8,128]{3,2,1,0:T(8,128)(2,1)}, bf16[288,8,8,128]{3,2,1,0:T(8,128)(2,1)S(1)}, u32[]{:S(2)}) copy-start(bf16[288,8,8,128]{3,2,1,0:T(8,128)(2,1)S(1)} %copy.171) | copy-start | bytes 14155780
  39.1 2.2 %copy-start.5 = (bf16[32,8,8,128]{3,2,1,0:T(8,128)(2,1)S(1)}, bf16[32,8,8,128]{3,2,1,0:T(8,128)(2,1)}, u32[]{:S(2)}) copy-start(bf16[32,8,8,128]{3,2,1,0:T(8,128)(2,1)} %copy.175) | copy-start | bytes 1572868
  83.8 4.5 %copy-start.3 = (bf16[4,8,64,576]{3,2,1,0:T(8,128)(2,1)S(1)}, bf16[4,8,64,576]{3,2,1,0:T(8,128)(2,1)}, u32[]{:S(2)}) copy-start(bf16[4,8,64,576]{3,2,1,0:T(8,128)(2,1)} %get-tuple-element.45) | copy-start | bytes 7077892
  85.5 107.9 %collective-permute-start.7 = (f32[256,1024]{1,0:T(8,128)}, f32[256,1024]{1,0:T(8,128)}, u32[]{:S(2)}, u32[]{:S(2)}) collective-permute-start(f32[256,1024]{1,0:T(8,128)} %bitcast.67), channel_id=1, source_target_pairs={{2,0},{3,1},{4,2},{5,3},{6,4},{7,5},{8,6},{9,7},{10,8},{11,9},{12,... | collective-permute-start | bytes 3145736 | tf_op jit(solution)/shard_map/ppermute | solution.py:14
  86.8 106.6 %collective-permute-start.6 = (f32[256,1024]{1,0:T(8,128)}, f32[256,1024]{1,0:T(8,128)}, u32[]{:S(2)}, u32[]{:S(2)}) collective-permute-start(f32[256,1024]{1,0:T(8,128)} %bitcast.66), channel_id=1, source_target_pairs={{1,0},{2,1},{3,2},{4,3},{5,4},{6,5},{7,6},{8,7},{9,8},{10,9},{11,1... | collective-permute-start | bytes 3145736 | tf_op jit(solution)/shard_map/ppermute | solution.py:14
  110.0 10.2 %slice-start = ((s8[4718592]{0:T(1024)(128)(4,1)}), s8[524288]{0:T(1024)(128)(4,1)S(1)}, s32[]{:S(2)}) async-start(s8[4718592]{0:T(1024)(128)(4,1)} %bitcast.210), calls=%async_computation | async-start | bytes 1048576
  114.8 5.4 %slice-start.1 = ((s8[4718592]{0:T(1024)(128)(4,1)}), s8[4194304]{0:T(1024)(128)(4,1)S(1)}, s32[]{:S(2)}) async-start(s8[4718592]{0:T(1024)(128)(4,1)} %bitcast.210), calls=%async_computation.1 | async-start | bytes 8388608
  115.8 4.4 %copy-start.4 = (bf16[4,8,64,576]{3,2,1,0:T(8,128)(2,1)S(1)}, bf16[4,8,64,576]{3,2,1,0:T(8,128)(2,1)}, u32[]{:S(2)}) copy-start(bf16[4,8,64,576]{3,2,1,0:T(8,128)(2,1)} %get-tuple-element.45) | copy-start | bytes 7077892
  117.5 78.5 %collective-permute-start.5 = (f32[256,1024]{1,0:T(8,128)}, f32[256,1024]{1,0:T(8,128)S(1)}, u32[]{:S(2)}, u32[]{:S(2)}) collective-permute-start(f32[256,1024]{1,0:T(8,128)} %bitcast.54), channel_id=1, source_target_pairs={{2,0},{3,1},{4,2},{5,3},{6,4},{7,5},{8,6},{9,7},{10,8},{11,9},{12,... | collective-permute-start | bytes 3145736 | tf_op jit(solution)/shard_map/ppermute | solution.py:14
  118.9 77.1 %collective-permute-start.4 = (f32[256,1024]{1,0:T(8,128)}, f32[256,1024]{1,0:T(8,128)}, u32[]{:S(2)}, u32[]{:S(2)}) collective-permute-start(f32[256,1024]{1,0:T(8,128)} %bitcast.53), channel_id=1, source_target_pairs={{1,0},{2,1},{3,2},{4,3},{5,4},{6,5},{7,6},{8,7},{9,8},{10,9},{11,1... | collective-permute-start | bytes 3145736 | tf_op jit(solution)/shard_map/ppermute | solution.py:14
  120.2 78.0 %copy-start.1 = (f32[8,320]{1,0:T(8,128)S(1)}, f32[8,320]{1,0:T(8,128)}, u32[]{:S(2)}) copy-start(f32[8,320]{1,0:T(8,128)} %param.13) | copy-start | bytes 30724
where the time goes:
time: 200 us; the launch traced here: 198 us
  local copies, waits for them, and re-layouts  81.9 us (41%)
  blocking collectives  70.2 us (35%)
  starting transfers between devices  19.5 us (10%)
  matrix products  14.8 us (7%)
  other arithmetic  7.04 us (4%)
  waiting for transfers between devices  3.66 us (2%)
    psum x1, blocking collectives, local(): grad_table = lax.psum(tap_part, ('sp', 'tp'))  70.2 us
    unnamed x52, local copies, waits for them, and re-layouts  19.8 us
    ppermute x8, starting transfers between devices, passed_along(): return lax.ppermute(block, axis, route)  19.5 us
    transpose x1, local copies, waits for them, and re-layouts, local(): jnp.einsum('bhqk,bqhd->bkhd', weights_b, grad_heads, preferred_element_ty...  12.8 us
    reshape x1, local copies, waits for them, and re-layouts, local(): value_band_grad.reshape(seg_count, span_segs, SEG_LEN, feature_count)  11.2 us
    reshape x1, local copies, waits for them, and re-layouts, local(): (key_band_grad * inv_root).reshape(seg_count, span_segs, SEG_LEN, feature...  11.1 us
    mul x1, local copies, waits for them, and re-layouts, local(): key_band_grad * inv_root  9.13 us
    dot_general x1, matrix products, local(): jnp.einsum('bhqk,bqhd->bkhd', weights_b, grad_heads, preferred_element_ty...  5.01 us
  transfers between devices with their start and end apart: 8, of which 1 were waited for; matrix products, arithmetic and copies ran while one was open for 23% of the time, Pallas kernels for 0%

commit v1 on v0

v1 whole, which is shorter than its diff:
```python
import functools
import math

import jax
import jax.numpy as jnp
from jax import lax
from jax.experimental import pallas as pl
from jax.experimental.pallas import tpu as pltpu
from jax.sharding import PartitionSpec as P

SEG_LEN = 64
LEFT_SEGS = 8
REL_CLIP = 256
AXES = ("sp", "tp")
LOG2E = math.log2(math.e)
MASKED = -1e30
F32 = jnp.float32
BF16 = jnp.bfloat16
NT = (((1,), (1,)), ((), ()))
NN = (((1,), (0,)), ((), ()))
TN = (((0,), (0,)), ((), ()))


def shifted(block, distance):
    count = lax.axis_size(AXES)
    route = [(i - distance, i) for i in range(count) if 0 <= i - distance < count]
    return lax.ppermute(block, AXES, route)


def prime_radices(count):
    radices = []
    twos = 0
    while count % 2 == 0:
        count //= 2
        twos += 1
    while twos > 0:
        take = 2 if twos != 3 else 3
        take = min(take, twos)
        radices.append(2**take)
        twos -= take
    factor = 3
    while count > 1:
        while count % factor == 0:
            radices.append(factor)
            count //= factor
        factor += 2
    return radices


def pair_tree(parts):
    while len(parts) > 1:
        parts = [parts[i] + parts[i + 1] for i in range(0, len(parts), 2)]
    return parts[0]


def all_sum(part):
    count = lax.axis_size(AXES)
    me = lax.axis_index(AXES)
    stride = 1
    for radix in prime_radices(count):
        if radix & (radix - 1) == 0:
            parts = [part]
            for step in range(1, radix):
                route = [(i, i ^ (step * stride)) for i in range(count)]
                parts.append(lax.ppermute(part, AXES, route))
            part = pair_tree(parts)
        else:
            digit = (me // stride) % radix
            parts = [part]
            for step in range(1, radix):
                route = []
                for i in range(count):
                    d = (i // stride) % radix
                    route.append((i, i + (((d - step) % radix) - d) * stride))
                parts.append(lax.ppermute(part, AXES, route))
            total = jnp.zeros_like(part)
            for d in range(radix):
                value = parts[0]
                for step in range(1, radix):
                    value = jnp.where((digit + step) % radix == d, parts[step], value)
                total = total + value
            part = total
        stride *= radix
    return part


def bias_kernel(chunk_ref, tile_ref):
    size = chunk_ref.shape[2]
    row = lax.broadcasted_iota(jnp.int32, (size, size), 0)
    col = lax.broadcasted_iota(jnp.int32, (size, size), 1)
    rolled = []
    for c in range(4):
        line = jnp.broadcast_to(chunk_ref[0, c : c + 1, :] * LOG2E, (size, size))
        rolled.append(pltpu.roll(line, 0, 1, stride=1, stride_axis=0))
    for b in range(3):
        tile = jnp.where(col >= row, rolled[b + 1], rolled[b])
        if b == 0:
            tile = jnp.where((row // SEG_LEN) <= (col // SEG_LEN), tile, MASKED)
        tile_ref[0, b] = tile


def unroll_sum(tile):
    size = tile.shape[0]
    group = 8
    parts = []
    for start in range(0, size, group):
        part = tile[start : start + group, :]
        parts.append(part if start == 0 else pltpu.roll(part, size - start, 1))
    total = pair_tree(parts)
    row = lax.broadcasted_iota(jnp.int32, total.shape, 0)
    for bit in (1, 2, 4):
        total = jnp.where((row & bit) != 0, pltpu.roll(total, size - bit, 1), total)
    return jnp.sum(total, axis=0, keepdims=True)


def score_terms(lag, key, value, query, grad, log_row, dot_row, tiles, const, inv_root):
    rows = key.shape[0]
    half = rows // 2
    raw = lax.dot_general(key, query, NT, preferred_element_type=F32)
    wgt = lax.dot_general(value, grad, NT, preferred_element_type=F32)
    row = lax.broadcasted_iota(jnp.int32, (half, half), 0) // SEG_LEN
    col = lax.broadcasted_iota(jnp.int32, (half, half), 1) // SEG_LEN
    acc = [None, None, None, None]
    w_rows, s_rows = [], []
    for r in range(2):
        w_cols, s_cols = [], []
        for c in range(2):
            if (lag == 0 and r > c) or (lag == 2 and c > r):
                w_cols.append(jnp.zeros((half, half), BF16))
                s_cols.append(jnp.zeros((half, half), BF16))
                continue
            rs, cs = slice(r * half, (r + 1) * half), slice(c * half, (c + 1) * half)
            level = min(2 * lag + c - r, 3)
            lrow = log_row[:, cs]
            bias = const - lrow if level == 3 else tiles[level] - lrow
            weight = jnp.exp2(raw[rs, cs] * (inv_root * LOG2E) + bias)
            if lag == 2 and r == c:
                weight = jnp.where(col <= row, weight, 0.0)
            score = weight * (wgt[rs, cs] - dot_row[:, cs])
            acc[level] = score if acc[level] is None else acc[level] + score
            w_cols.append(weight.astype(BF16))
            s_cols.append(score.astype(BF16))
        w_rows.append(jnp.concatenate(w_cols, axis=1))
        s_rows.append(jnp.concatenate(s_cols, axis=1))
    return jnp.concatenate(w_rows, axis=0), jnp.concatenate(s_rows, axis=0), acc


def table_lines(acc, size):
    row = lax.broadcasted_iota(jnp.int32, (size, size), 0)
    col = lax.broadcasted_iota(jnp.int32, (size, size), 1)
    lines = []
    for c in range(4):
        upper = acc[c - 1] if c > 0 else None
        lower = acc[c] if c < 3 else None
        line = None
        if upper is not None or lower is not None:
            zero = jnp.zeros((size, size), F32)
            mixed = jnp.where(
                col >= row,
                zero if upper is None else upper,
                zero if lower is None else lower,
            )
            line = unroll_sum(mixed)
        if c == 3 and acc[3] is not None:
            extra = jnp.sum(acc[3], axis=0, keepdims=True)
            line = extra if line is None else line + extra
        lines.append(jnp.zeros((1, size), F32) if line is None else line)
    return jnp.concatenate(lines, axis=0)


def lag_kernel(lag, heads_step, head_count, split, *refs):
    if lag == 0:
        (k_ref, v_ref, q_ref, g_ref, st_ref, tile_ref, chunk_ref, dq_ref, dk_ref, dv_ref, tab_ref) = refs
    elif not split:
        (k_ref, v_ref, q_ref, g_ref, st_ref, tile_ref, chunk_ref, dk_in, dv_in, tab_in,
         dq_ref, dk_ref, dv_ref, tab_ref) = refs
    else:
        (k_ref, v_ref, q_ref, g_ref, st_ref, tile_ref, chunk_ref, tab_in,
         dq_ref, tab_ref, w_ref, s_ref) = refs
    size = chunk_ref.shape[2]
    head_dim = k_ref.shape[1] // heads_step
    inv_root = head_dim ** (-0.5)
    step = pl.program_id(0)
    for i in range(heads_step):
        head = step * heads_step + i
        cols = slice(i * head_dim, (i + 1) * head_dim)
        key, value, query, grad = k_ref[:, cols], v_ref[:, cols], q_ref[:, cols], g_ref[:, cols]
        log_row = st_ref[pl.ds(head, 1), :]
        dot_row = st_ref[pl.ds(head + head_count, 1), :]
        const = chunk_ref[i, 3:4, :] * LOG2E
        tiles = [None if lag == 2 else tile_ref[i, b] for b in range(3)]
        weights, scores, acc = score_terms(
            lag, key, value, query, grad, log_row, dot_row, tiles, const, inv_root
        )
        dq = lax.dot_general(scores, key, TN, preferred_element_type=F32) * inv_root
        dq_ref[:, cols] = dq.astype(dq_ref.dtype)
        lines = table_lines(acc, size)
        tab_ref[i] = lines if lag == 0 else lines + tab_in[i]
        if split:
            w_ref[i] = weights
            s_ref[i] = scores
        else:
            dk = lax.dot_general(scores, query, NN, preferred_element_type=F32)
            dv = lax.dot_general(weights, grad, NN, preferred_element_type=F32)
            dk_ref[:, cols] = dk if lag == 0 else dk + dk_in[:, cols]
            dv_ref[:, cols] = dv if lag == 0 else dv + dv_in[:, cols]


def close_kernel(heads_step, w_ref, s_ref, q_ref, g_ref, dk_in, dv_in, dk_ref, dv_ref):
    head_dim = q_ref.shape[1] // heads_step
    inv_root = head_dim ** (-0.5)
    for i in range(heads_step):
        cols = slice(i * head_dim, (i + 1) * head_dim)
        dk = lax.dot_general(s_ref[i], q_ref[:, cols], NN, preferred_element_type=F32)
        dv = lax.dot_general(w_ref[i], g_ref[:, cols], NN, preferred_element_type=F32)
        dk_ref[:, cols] = ((dk + dk_in[:, cols]) * inv_root).astype(BF16)
        dv_ref[:, cols] = (dv + dv_in[:, cols]).astype(BF16)


def local(query_rows, key_rows, value_rows, out_grad, log_totals, out_dot, bias_table):
    rows, feats = query_rows.shape
    heads = log_totals.shape[1]
    table_len = bias_table.shape[1]
    half = rows // 2
    heads_step = 2
    grid = (heads // heads_step,)
    wide = feats // heads * heads_step
    lags = LEFT_SEGS * SEG_LEN // rows

    stats = jnp.concatenate([log_totals * LOG2E, out_dot], axis=1).T

    moved = {}
    for lag in range(1, lags + 1):
        moved[lag] = (shifted(query_rows, -lag), shifted(out_grad, -lag), shifted(stats, -lag))

    left_pad = 2 * half - REL_CLIP + half - SEG_LEN + 1
    padded = jnp.pad(bias_table, ((0, 0), (left_pad, 4 * half - left_pad - table_len)), mode="edge")
    chunks = padded.reshape(heads, 4, half)

    row_spec = pl.BlockSpec((rows, wide), lambda h: (0, h))
    stat_spec = pl.BlockSpec(stats.shape, lambda h: (0, 0))
    chunk_spec = pl.BlockSpec((heads_step, 4, half), lambda h: (h, 0, 0))
    tile_spec = pl.BlockSpec((heads_step, 3, half, half), lambda h: (h, 0, 0, 0))
    sq_spec = pl.BlockSpec((heads_step, rows, rows), lambda h: (h, 0, 0))
    rows_f32 = jax.ShapeDtypeStruct((rows, feats), F32)
    rows_b16 = jax.ShapeDtypeStruct((rows, feats), BF16)
    tab_shape = jax.ShapeDtypeStruct((heads, 4, half), F32)
    sq_shape = jax.ShapeDtypeStruct((heads, rows, rows), BF16)
    pair_flops = 2 * rows * rows * feats

    def cost(matmuls, size):
        return pl.CostEstimate(
            flops=matmuls * pair_flops, bytes_accessed=size, transcendentals=heads * rows * rows
        )

    tiles = pl.pallas_call(
        bias_kernel,
        grid=(heads,),
        in_specs=[pl.BlockSpec((1, 4, half), lambda h: (h, 0, 0))],
        out_specs=pl.BlockSpec((1, 3, half, half), lambda h: (h, 0, 0, 0)),
        out_shape=jax.ShapeDtypeStruct((heads, 3, half, half), F32),
        cost_estimate=cost(1, heads * 3 * half * half * 4),
        name="bias_tiles",
    )(chunks)

    base_specs = [row_spec] * 4 + [stat_spec, tile_spec, chunk_spec]
    body = functools.partial
    dq0, dk, dv, tab = pl.pallas_call(
        body(lag_kernel, 0, heads_step, heads, False),
        grid=grid,
        in_specs=base_specs,
        out_specs=[row_spec] * 3 + [chunk_spec],
        out_shape=[rows_f32] * 3 + [tab_shape],
        cost_estimate=cost(5, 8 * rows * feats),
        name="lag0",
    )(key_rows, value_rows, query_rows, out_grad, stats, tiles, chunks)

    dq2, dk, dv, tab = pl.pallas_call(
        body(lag_kernel, 2, heads_step, heads, False),
        grid=grid,
        in_specs=base_specs + [row_spec] * 2 + [chunk_spec],
        out_specs=[row_spec] * 3 + [chunk_spec],
        out_shape=[rows_b16] + [rows_f32] * 2 + [tab_shape],
        cost_estimate=cost(5, 8 * rows * feats),
        name="lag2",
    )(key_rows, value_rows, *moved[2], tiles, chunks, dk, dv, tab)
    back2 = shifted(dq2, 2)

    dq1, tab, weights, scores = pl.pallas_call(
        body(lag_kernel, 1, heads_step, heads, True),
        grid=grid,
        in_specs=base_specs + [chunk_spec],
        out_specs=[row_spec, chunk_spec, sq_spec, sq_spec],
        out_shape=[rows_b16, tab_shape, sq_shape, sq_shape],
        cost_estimate=cost(3, 8 * rows * feats),
        name="lag1",
    )(key_rows, value_rows, *moved[1], tiles, chunks, tab)
    back1 = shifted(dq1, 1)

    grad_key, grad_value = pl.pallas_call(
        body(close_kernel, heads_step),
        grid=grid,
        in_specs=[sq_spec, sq_spec] + [row_spec] * 4,
        out_specs=[row_spec] * 2,
        out_shape=[rows_b16] * 2,
        cost_estimate=cost(2, 8 * rows * feats),
        name="close",
    )(weights, scores, moved[1][0], moved[1][1], dk, dv)

    lines = all_sum(tab.reshape(heads, 4 * half))
    grad_table = jnp.concatenate(
        [
            lines[:, left_pad : left_pad + table_len - 1],
            jnp.sum(lines[:, left_pad + table_len - 1 :], axis=1, keepdims=True),
        ],
        axis=1,
    )
    grad_query = (dq0 + back1.astype(F32) + back2.astype(F32)).astype(BF16)
    return grad_query, grad_key, grad_value, grad_table


def solution(mesh):
    placed = (P(AXES, None),) * 6 + (P(),)
    return jax.shard_map(
        local,
        mesh=mesh,
        in_specs=placed,
        out_specs=(P(AXES, None),) * 3 + (P(),),
        check_vma=False,
    )
```

time: 200 us -> 82.7 us (0.41)
  the two profiles are of different devices: /device:TPU:0 before, /device:TPU:3 now
where the time goes in v1:
time: 82.7 us; the launch traced here: 81.7 us
  starting transfers between devices  41.2 us (50%)
  Pallas kernels  28.6 us (35%)
  other arithmetic  4.76 us (6%)
  local copies, waits for them, and re-layouts  4.43 us (5%)
  waiting for transfers between devices  1.79 us (2%)
  between operations  0.89 us (1%)
    ppermute x8, starting transfers between devices, shifted(): return lax.ppermute(block, AXES, route)  24.1 us
    ppermute x10, starting transfers between devices, all_sum(): parts.append(lax.ppermute(part, AXES, route))  17.2 us
    pallas_call x1, Pallas kernels, local(): pl.pallas_call(body(lag_kernel, 0, heads_step, heads, False), grid=grid,...  6.54 us
    pallas_call x1, Pallas kernels, local(): pl.pallas_call(body(lag_kernel, 2, heads_step, heads, False), grid=grid,...  6.46 us
    pallas_call x1, Pallas kernels, local(): pl.pallas_call(body(lag_kernel, 1, heads_step, heads, True), grid=grid, i...  6.24 us
    pallas_call x1, Pallas kernels, local(): pl.pallas_call(body(close_kernel, heads_step), grid=grid, in_specs=[sq_sp...  4.73 us
    pallas_call x1, Pallas kernels, local(): pl.pallas_call(bias_kernel, grid=(heads,), in_specs=[pl.BlockSpec((1, 4,...  4.62 us
    unnamed x19, local copies, waits for them, and re-layouts  2.6 us
  transfers between devices with their start and end apart: 18, of which 2 were waited for; matrix products, arithmetic and copies ran while one was open for 7% of the time, Pallas kernels for 27%

profile of v1, /device:TPU:3, one launch (start us, length us, event | category | flops | bytes accessed | tf_op | source)
XLA Modules:
  0.0 81.7 jit_solution(16997262360172180997)
XLA Ops:
  0.6 2.6 %collective-permute-start.3 = (bf16[256,1024]{1,0:T(8,128)(2,1)}, bf16[256,1024]{1,0:T(8,128)(2,1)S(1)}, u32[]{:S(2)}, u32[]{:S(2)}) collective-permute-start(bf16[256,1024]{1,0:T(8,128)(2,1)} %refs_2_.1), channel_id=1, source_target_pairs={{2,0},{3,1},{4,2},{5,3},{6,4},{7,5},{8,6},{9,7},{10,8},{11,9},{12,... | collective-permute-start | bytes 1572872 | tf_op jit(solution)/shard_map/ppermute | solution.py:27
  3.2 1.9 %collective-permute-start = (bf16[256,1024]{1,0:T(8,128)(2,1)}, bf16[256,1024]{1,0:T(8,128)(2,1)S(1)}, u32[]{:S(2)}, u32[]{:S(2)}) collective-permute-start(bf16[256,1024]{1,0:T(8,128)(2,1)} %refs_2_.1), channel_id=1, source_target_pairs={{1,0},{2,1},{3,2},{4,3},{5,4},{6,5},{7,6},{8,7},{9,8},{10,9},{11,1... | collective-permute-start | bytes 1572872 | tf_op jit(solution)/shard_map/ppermute | solution.py:27
  5.2 1.9 %collective-permute-start.4 = (bf16[256,1024]{1,0:T(8,128)(2,1)}, bf16[256,1024]{1,0:T(8,128)(2,1)S(1)}, u32[]{:S(2)}, u32[]{:S(2)}) collective-permute-start(bf16[256,1024]{1,0:T(8,128)(2,1)} %refs_3_.1), channel_id=1, source_target_pairs={{2,0},{3,1},{4,2},{5,3},{6,4},{7,5},{8,6},{9,7},{10,8},{11,9},{12,... | collective-permute-start | bytes 1572872 | tf_op jit(solution)/shard_map/ppermute | solution.py:27
  7.1 2.6 %collective-permute-start.1 = (bf16[256,1024]{1,0:T(8,128)(2,1)}, bf16[256,1024]{1,0:T(8,128)(2,1)S(1)}, u32[]{:S(2)}, u32[]{:S(2)}) collective-permute-start(bf16[256,1024]{1,0:T(8,128)(2,1)} %refs_3_.1), channel_id=1, source_target_pairs={{1,0},{2,1},{3,2},{4,3},{5,4},{6,5},{7,6},{8,7},{9,8},{10,9},{11,1... | collective-permute-start | bytes 1572872 | tf_op jit(solution)/shard_map/ppermute | solution.py:27
  9.7 0.7 broadcast_multiply_fusion
  10.4 0.7 maximum_bitcast_fusion.refs_4_
  11.1 1.9 %collective-permute-start.5 = (f32[16,256]{1,0:T(8,128)S(1)}, f32[16,256]{1,0:T(8,128)S(1)}, u32[]{:S(2)}, u32[]{:S(2)}) collective-permute-start(f32[16,256]{1,0:T(8,128)S(1)} %maximum_bitcast_fusion.refs_4_), channel_id=1, source_target_pairs={{2,0},{3,1},{4,2},{5,3},{6,4},{7,5},{8,6},{9,7},{10,8},{11,9},{12,... | collective-permute-start | bytes 49160 | tf_op jit(solution)/shard_map/ppermute | solution.py:27
  13.0 0.9 %slice_reduce_fusion.2 = (f32[8]{0:T(128)S(1)}, f32[8]{0:T(128)S(1)}) fusion(f32[8,320]{1,0:T(8,128)} %param.13), kind=kLoop, calls=%fused_computation.9 | loop fusion | bytes 128 | tf_op jit(solution)/shard_map/jit(_pad)/slice | solution.py:237
  14.1 0.8 pad_maximum_fusion
  14.9 0.6 reshape.26.chunk_ref.refs_6_
  15.5 4.6 %bias_tiles.1.refs_5_ = f32[8,3,128,128]{3,2,1,0:T(8,128)} custom-call(f32[8,4,128]{2,1,0:T(4,128)} %reshape.26.chunk_ref.refs_6_), custom_call_target="tpu_custom_call" | custom-call | flops 134217728 | bytes 1572864 | tf_op jit(solution)/shard_map/bias_tiles/pallas_call | solution.py:256
  20.1 6.5 %lag0.1 = (f32[256,1024]{1,0:T(8,128)}, f32[256,1024]{1,0:T(8,128)}, f32[256,1024]{1,0:T(8,128)}, f32[8,4,128]{2,1,0:T(4,128)}) custom-call(bf16[256,1024]{1,0:T(8,128)(2,1)} %refs_0_.5, bf16[256,1024]{1,0:T(8,128)(2,1)} %refs_1_.5, bf16[256,1024]{1,0:T(8,128)(2,1)} %refs_2_.1, bf16[256,1024]{1,0:T(8,128)(2,1)} %refs_3_.1, f32[16,256]{1,0:T(8,128)} %copy-done.5, ...), custom_call_target="tpu_custom_call" | custom-call | flops 671088640 | bytes 2097152 | tf_op jit(solution)/shard_map/lag0/pallas_call | solution.py:268
  26.7 1.9 %collective-permute-start.2 = (f32[16,256]{1,0:T(8,128)}, f32[16,256]{1,0:T(8,128)S(1)}, u32[]{:S(2)}, u32[]{:S(2)}) collective-permute-start(f32[16,256]{1,0:T(8,128)} %copy-done.5), channel_id=1, source_target_pairs={{1,0},{2,1},{3,2},{4,3},{5,4},{6,5},{7,6},{8,7},{9,8},{10,9},{11,1... | collective-permute-start | bytes 49160 | tf_op jit(solution)/shard_map/ppermute | solution.py:27
  28.7 0.8 copy-done.3
  29.6 6.5 %lag2.1 = (bf16[256,1024]{1,0:T(8,128)(2,1)}, f32[256,1024]{1,0:T(8,128)}, f32[256,1024]{1,0:T(8,128)}, f32[8,4,128]{2,1,0:T(4,128)}) custom-call(bf16[256,1024]{1,0:T(8,128)(2,1)} %refs_0_.5, bf16[256,1024]{1,0:T(8,128)(2,1)} %refs_1_.5, bf16[256,1024]{1,0:T(8,128)(2,1)} %copy-done.3, bf16[256,1024]{1,0:T(8,128)(2,1)} %copy-done.4, f32[16,256]{1,0:T(8,128)} %copy-done.6, ...), custom_call_target="tpu_custom_call" | custom-call | flops 671088640 | bytes 2097152 | tf_op jit(solution)/shard_map/lag2/pallas_call | solution.py:278
  36.1 0.6 copy-done.7
  37.1 6.2 %lag1.1 = (bf16[256,1024]{1,0:T(8,128)(2,1)}, f32[8,4,128]{2,1,0:T(4,128)}, bf16[8,256,256]{2,1,0:T(8,128)(2,1)}, bf16[8,256,256]{2,1,0:T(8,128)(2,1)}) custom-call(bf16[256,1024]{1,0:T(8,128)(2,1)} %refs_0_.5, bf16[256,1024]{1,0:T(8,128)(2,1)} %refs_1_.5, bf16[256,1024]{1,0:T(8,128)(2,1)} %copy-done, bf16[256,1024]{1,0:T(8,128)(2,1)} %copy-done.1, ...), custom_call_target="tpu_custom_call" | custom-call | flops 402653184 | bytes 2097152 | tf_op jit(solution)/shard_map/lag1/pallas_call | solution.py:289
  43.3 0.7 copy.16
  44.4 1.5 %collective-permute-start.8 = (f32[8,512]{1,0:T(8,128)S(1)}, f32[8,512]{1,0:T(8,128)S(1)}, u32[]{:S(2)}, u32[]{:S(2)}) collective-permute-start(f32[8,512]{1,0:T(8,128)S(1)} %bitcast.13), channel_id=1, source_target_pairs={{0,1},{1,0},{2,3},{3,2},{4,5},{5,4},{6,7},{7,6},{8,9},{9,8},{10,11... | collective-permute-start | bytes 49160 | tf_op jit(solution)/shard_map/ppermute | solution.py:65
  45.9 9.3 %collective-permute-start.7 = (bf16[256,1024]{1,0:T(8,128)(2,1)S(1)}, bf16[256,1024]{1,0:T(8,128)(2,1)S(1)}, u32[]{:S(2)}, u32[]{:S(2)}) collective-permute-start(bf16[256,1024]{1,0:T(8,128)(2,1)S(1)} %copy-done.8), channel_id=1, source_target_pairs={{0,2},{1,3},{2,4},{3,5},{4,6},{5,7},{6,8},{7,9},{8,10},{9,11},{10,... | collective-permute-start | bytes 1572872 | tf_op jit(solution)/shard_map/ppermute | solution.py:27
  55.1 1.9 %collective-permute-start.6 = (bf16[256,1024]{1,0:T(8,128)(2,1)}, bf16[256,1024]{1,0:T(8,128)(2,1)S(1)}, u32[]{:S(2)}, u32[]{:S(2)}) collective-permute-start(bf16[256,1024]{1,0:T(8,128)(2,1)} %get-tuple-element.23), channel_id=1, source_target_pairs={{0,1},{1,2},{2,3},{3,4},{4,5},{5,6},{6,7},{7,8},{8,9},{9,10},{10,1... | collective-permute-start | bytes 1572872 | tf_op jit(solution)/shard_map/ppermute | solution.py:27
  57.1 0.7 add_add_fusion.1
  57.8 1.3 %collective-permute-start.16 = (f32[8,512]{1,0:T(8,128)S(1)}, f32[8,512]{1,0:T(8,128)S(1)}, u32[]{:S(2)}, u32[]{:S(2)}) collective-permute-start(f32[8,512]{1,0:T(8,128)S(1)} %add_add_fusion.1), channel_id=1, source_target_pairs={{0,24},{1,25},{2,26},{3,27},{4,28},{5,29},{6,30},{7,31},{8,16},{9,... | collective-permute-start | bytes 49160 | tf_op jit(solution)/shard_map/ppermute | solution.py:65
  59.1 1.9 %collective-permute-start.17 = (f32[8,512]{1,0:T(8,128)S(1)}, f32[8,512]{1,0:T(8,128)S(1)}, u32[]{:S(2)}, u32[]{:S(2)}) collective-permute-start(f32[8,512]{1,0:T(8,128)S(1)} %add_add_fusion.1), channel_id=1, source_target_pairs={{0,28},{1,29},{2,30},{3,31},{4,24},{5,25},{6,26},{7,27},{8,20},{9,... | collective-permute-start | bytes 49160 | tf_op jit(solution)/shard_map/ppermute | solution.py:65
  61.0 0.5 collective-permute-start.14
  61.5 0.7 collective-permute-done.16
  62.2 10.0 %collective-permute-start.15 = (f32[8,512]{1,0:T(8,128)S(1)}, f32[8,512]{1,0:T(8,128)S(1)}, u32[]{:S(2)}, u32[]{:S(2)}) collective-permute-start(f32[8,512]{1,0:T(8,128)S(1)} %add_add_fusion.1), channel_id=1, source_target_pairs={{0,20},{1,21},{2,22},{3,23},{4,16},{5,17},{6,18},{7,19},{8,28},{9,... | collective-permute-start | bytes 49160 | tf_op jit(solution)/shard_map/ppermute | solution.py:65
  72.4 1.0 %collective-permute-done.15 = f32[8,512]{1,0:T(8,128)S(1)} collective-permute-done((f32[8,512]{1,0:T(8,128)S(1)}, f32[8,512]{1,0:T(8,128)S(1)}, u32[]{:S(2)}, u32[]{:S(2)}) %collective-permute-start.15) | collective-permute-done | bytes 16416 | tf_op jit(solution)/shard_map/ppermute | solution.py:65
  73.4 1.5 %collective-permute-start.11 = (f32[8,512]{1,0:T(8,128)S(1)}, f32[8,512]{1,0:T(8,128)S(1)}, u32[]{:S(2)}, u32[]{:S(2)}) collective-permute-start(f32[8,512]{1,0:T(8,128)S(1)} %add_add_fusion.1), channel_id=1, source_target_pairs={{0,4},{1,5},{2,6},{3,7},{4,0},{5,1},{6,2},{7,3},{8,12},{9,13},{10,... | collective-permute-start | bytes 49160 | tf_op jit(solution)/shard_map/ppermute | solution.py:65
  74.9 4.7 %close.1 = (bf16[256,1024]{1,0:T(8,128)(2,1)}, bf16[256,1024]{1,0:T(8,128)(2,1)}) custom-call(bf16[8,256,256]{2,1,0:T(8,128)(2,1)} %get-tuple-element.25.w_ref, bf16[8,256,256]{2,1,0:T(8,128)(2,1)} %get-tuple-element.26.s_ref, bf16[256,1024]{1,0:T(8,128)(2,1)} %copy-done, bf16[256,1024]{1,0:T(8,128)(2,1)} %copy-done.1, f32[256,1024]{1,0:T(8,128)} %get-tuple-element.27.dk_in, ...), custom_call_target="tpu_custom_call" | custom-call | flops 268435456 | bytes 2097152 | tf_op jit(solution)/shard_map/close/pallas_call | solution.py:300
  80.0 0.7 pad_maximum_fusion.1
  80.7 1.0 %add_convert_fusion = bf16[256,1024]{1,0:T(8,128)(2,1)} fusion(bf16[256,1024]{1,0:T(8,128)(2,1)S(1)} %collective-permute-done.7, f32[256,1024]{1,0:T(8,128)S(1)} %copy-done.2, bf16[256,1024]{1,0:T(8,128)(2,1)S(1)} %collective-permute-done.6), kind=kLoop, calls=%fused_computation | loop fusion | flops 1310720 | bytes 2621440 | tf_op jit(solution)/shard_map/convert_element_type | solution.py:318
  (42 shorter events, 1.5 us)
Async XLA Ops:
  0.6 28.0 %collective-permute-start.3 = (bf16[256,1024]{1,0:T(8,128)(2,1)}, bf16[256,1024]{1,0:T(8,128)(2,1)S(1)}, u32[]{:S(2)}, u32[]{:S(2)}) collective-permute-start(bf16[256,1024]{1,0:T(8,128)(2,1)} %refs_2_.1), channel_id=1, source_target_pairs={{2,0},{3,1},{4,2},{5,3},{6,4},{7,5},{8,6},{9,7},{10,8},{11,9},{12,... | collective-permute-start | bytes 1572872 | tf_op jit(solution)/shard_map/ppermute | solution.py:27
  3.2 32.9 %collective-permute-start = (bf16[256,1024]{1,0:T(8,128)(2,1)}, bf16[256,1024]{1,0:T(8,128)(2,1)S(1)}, u32[]{:S(2)}, u32[]{:S(2)}) collective-permute-start(bf16[256,1024]{1,0:T(8,128)(2,1)} %refs_2_.1), channel_id=1, source_target_pairs={{1,0},{2,1},{3,2},{4,3},{5,4},{6,5},{7,6},{8,7},{9,8},{10,9},{11,1... | collective-permute-start | bytes 1572872 | tf_op jit(solution)/shard_map/ppermute | solution.py:27
  5.2 23.5 %collective-permute-start.4 = (bf16[256,1024]{1,0:T(8,128)(2,1)}, bf16[256,1024]{1,0:T(8,128)(2,1)S(1)}, u32[]{:S(2)}, u32[]{:S(2)}) collective-permute-start(bf16[256,1024]{1,0:T(8,128)(2,1)} %refs_3_.1), channel_id=1, source_target_pairs={{2,0},{3,1},{4,2},{5,3},{6,4},{7,5},{8,6},{9,7},{10,8},{11,9},{12,... | collective-permute-start | bytes 1572872 | tf_op jit(solution)/shard_map/ppermute | solution.py:27
  7.1 29.0 %collective-permute-start.1 = (bf16[256,1024]{1,0:T(8,128)(2,1)}, bf16[256,1024]{1,0:T(8,128)(2,1)S(1)}, u32[]{:S(2)}, u32[]{:S(2)}) collective-permute-start(bf16[256,1024]{1,0:T(8,128)(2,1)} %refs_3_.1), channel_id=1, source_target_pairs={{1,0},{2,1},{3,2},{4,3},{5,4},{6,5},{7,6},{8,7},{9,8},{10,9},{11,1... | collective-permute-start | bytes 1572872 | tf_op jit(solution)/shard_map/ppermute | solution.py:27
  11.1 9.0 %copy-start.5 = (f32[16,256]{1,0:T(8,128)}, f32[16,256]{1,0:T(8,128)S(1)}, u32[]{:S(2)}) copy-start(f32[16,256]{1,0:T(8,128)S(1)} %maximum_bitcast_fusion.refs_4_) | copy-start | bytes 49156
  11.1 15.5 %collective-permute-start.5 = (f32[16,256]{1,0:T(8,128)S(1)}, f32[16,256]{1,0:T(8,128)S(1)}, u32[]{:S(2)}, u32[]{:S(2)}) collective-permute-start(f32[16,256]{1,0:T(8,128)S(1)} %maximum_bitcast_fusion.refs_4_), channel_id=1, source_target_pairs={{2,0},{3,1},{4,2},{5,3},{6,4},{7,5},{8,6},{9,7},{10,8},{11,9},{12,... | collective-permute-start | bytes 49160 | tf_op jit(solution)/shard_map/ppermute | solution.py:27
  26.7 2.0 %copy-start.6 = (f32[16,256]{1,0:T(8,128)}, f32[16,256]{1,0:T(8,128)S(1)}, u32[]{:S(2)}) copy-start(f32[16,256]{1,0:T(8,128)S(1)} %collective-permute-done.5.refs_4_) | copy-start | bytes 49156
  26.7 9.4 %collective-permute-start.2 = (f32[16,256]{1,0:T(8,128)}, f32[16,256]{1,0:T(8,128)S(1)}, u32[]{:S(2)}, u32[]{:S(2)}) collective-permute-start(f32[16,256]{1,0:T(8,128)} %copy-done.5), channel_id=1, source_target_pairs={{1,0},{2,1},{3,2},{4,3},{5,4},{6,5},{7,6},{8,7},{9,8},{10,9},{11,1... | collective-permute-start | bytes 49160 | tf_op jit(solution)/shard_map/ppermute | solution.py:27
  28.6 0.8 copy-start.3
  28.6 0.9 %copy-start.4 = (bf16[256,1024]{1,0:T(8,128)(2,1)}, bf16[256,1024]{1,0:T(8,128)(2,1)S(1)}, u32[]{:S(2)}) copy-start(bf16[256,1024]{1,0:T(8,128)(2,1)S(1)} %collective-permute-done.4.refs_3_) | copy-start | bytes 1572868
  36.1 0.6 copy-start.7
  36.1 0.8 copy-start
  36.1 0.9 %copy-start.1 = (bf16[256,1024]{1,0:T(8,128)(2,1)}, bf16[256,1024]{1,0:T(8,128)(2,1)S(1)}, u32[]{:S(2)}) copy-start(bf16[256,1024]{1,0:T(8,128)(2,1)S(1)} %collective-permute-done.1.refs_3_.g_ref) | copy-start | bytes 1572868
  37.1 8.8 %copy-start.8 = (bf16[256,1024]{1,0:T(8,128)(2,1)S(1)}, bf16[256,1024]{1,0:T(8,128)(2,1)}, u32[]{:S(2)}) copy-start(bf16[256,1024]{1,0:T(8,128)(2,1)} %get-tuple-element.24) | copy-start | bytes 1572868
  44.0 13.1 %collective-permute-start.9 = (f32[8,512]{1,0:T(8,128)S(1)}, f32[8,512]{1,0:T(8,128)S(1)}, u32[]{:S(2)}, u32[]{:S(2)}) collective-permute-start(f32[8,512]{1,0:T(8,128)S(1)} %bitcast.11), channel_id=1, source_target_pairs={{0,2},{1,3},{2,0},{3,1},{4,6},{5,7},{6,4},{7,5},{8,10},{9,11},{10,... | collective-permute-start | bytes 49160 | tf_op jit(solution)/shard_map/ppermute | solution.py:65
  44.0 13.1 %collective-permute-start.10 = (f32[8,512]{1,0:T(8,128)S(1)}, f32[8,512]{1,0:T(8,128)S(1)}, u32[]{:S(2)}, u32[]{:S(2)}) collective-permute-start(f32[8,512]{1,0:T(8,128)S(1)} %bitcast.12), channel_id=1, source_target_pairs={{0,3},{1,2},{2,1},{3,0},{4,7},{5,6},{6,5},{7,4},{8,11},{9,10},{10,... | collective-permute-start | bytes 49160 | tf_op jit(solution)/shard_map/ppermute | solution.py:65
  44.4 12.7 %collective-permute-start.8 = (f32[8,512]{1,0:T(8,128)S(1)}, f32[8,512]{1,0:T(8,128)S(1)}, u32[]{:S(2)}, u32[]{:S(2)}) collective-permute-start(f32[8,512]{1,0:T(8,128)S(1)} %bitcast.13), channel_id=1, source_target_pairs={{0,1},{1,0},{2,3},{3,2},{4,5},{5,4},{6,7},{7,6},{8,9},{9,8},{10,11... | collective-permute-start | bytes 49160 | tf_op jit(solution)/shard_map/ppermute | solution.py:65
  45.9 34.8 %collective-permute-start.7 = (bf16[256,1024]{1,0:T(8,128)(2,1)S(1)}, bf16[256,1024]{1,0:T(8,128)(2,1)S(1)}, u32[]{:S(2)}, u32[]{:S(2)}) collective-permute-start(bf16[256,1024]{1,0:T(8,128)(2,1)S(1)} %copy-done.8), channel_id=1, source_target_pairs={{0,2},{1,3},{2,4},{3,5},{4,6},{5,7},{6,8},{7,9},{8,10},{9,11},{10,... | collective-permute-start | bytes 1572872 | tf_op jit(solution)/shard_map/ppermute | solution.py:27
  55.1 25.5 %collective-permute-start.6 = (bf16[256,1024]{1,0:T(8,128)(2,1)}, bf16[256,1024]{1,0:T(8,128)(2,1)S(1)}, u32[]{:S(2)}, u32[]{:S(2)}) collective-permute-start(bf16[256,1024]{1,0:T(8,128)(2,1)} %get-tuple-element.23), channel_id=1, source_target_pairs={{0,1},{1,2},{2,3},{3,4},{4,5},{5,6},{6,7},{7,8},{8,9},{9,10},{10,1... | collective-permute-start | bytes 1572872 | tf_op jit(solution)/shard_map/ppermute | solution.py:27
  57.8 4.4 %collective-permute-start.16 = (f32[8,512]{1,0:T(8,128)S(1)}, f32[8,512]{1,0:T(8,128)S(1)}, u32[]{:S(2)}, u32[]{:S(2)}) collective-permute-start(f32[8,512]{1,0:T(8,128)S(1)} %add_add_fusion.1), channel_id=1, source_target_pairs={{0,24},{1,25},{2,26},{3,27},{4,28},{5,29},{6,30},{7,31},{8,16},{9,... | collective-permute-start | bytes 49160 | tf_op jit(solution)/shard_map/ppermute | solution.py:65
  59.1 13.1 %collective-permute-start.17 = (f32[8,512]{1,0:T(8,128)S(1)}, f32[8,512]{1,0:T(8,128)S(1)}, u32[]{:S(2)}, u32[]{:S(2)}) collective-permute-start(f32[8,512]{1,0:T(8,128)S(1)} %add_add_fusion.1), channel_id=1, source_target_pairs={{0,28},{1,29},{2,30},{3,31},{4,24},{5,25},{6,26},{7,27},{8,20},{9,... | collective-permute-start | bytes 49160 | tf_op jit(solution)/shard_map/ppermute | solution.py:65
  61.0 11.2 %collective-permute-start.14 = (f32[8,512]{1,0:T(8,128)S(1)}, f32[8,512]{1,0:T(8,128)S(1)}, u32[]{:S(2)}, u32[]{:S(2)}) collective-permute-start(f32[8,512]{1,0:T(8,128)S(1)} %add_add_fusion.1), channel_id=1, source_target_pairs={{0,16},{1,17},{2,18},{3,19},{4,20},{5,21},{6,22},{7,23},{8,24},{9,... | collective-permute-start | bytes 49160 | tf_op jit(solution)/shard_map/ppermute | solution.py:65
  62.2 11.2 %collective-permute-start.15 = (f32[8,512]{1,0:T(8,128)S(1)}, f32[8,512]{1,0:T(8,128)S(1)}, u32[]{:S(2)}, u32[]{:S(2)}) collective-permute-start(f32[8,512]{1,0:T(8,128)S(1)} %add_add_fusion.1), channel_id=1, source_target_pairs={{0,20},{1,21},{2,22},{3,23},{4,16},{5,17},{6,18},{7,19},{8,28},{9,... | collective-permute-start | bytes 49160 | tf_op jit(solution)/shard_map/ppermute | solution.py:65
  72.3 7.4 %collective-permute-start.12 = (f32[8,512]{1,0:T(8,128)S(1)}, f32[8,512]{1,0:T(8,128)S(1)}, u32[]{:S(2)}, u32[]{:S(2)}) collective-permute-start(f32[8,512]{1,0:T(8,128)S(1)} %add_add_fusion.1), channel_id=1, source_target_pairs={{0,8},{1,9},{2,10},{3,11},{4,12},{5,13},{6,14},{7,15},{8,0},{9,1},... | collective-permute-start | bytes 49160 | tf_op jit(solution)/shard_map/ppermute | solution.py:65
  72.3 7.4 %collective-permute-start.13 = (f32[8,512]{1,0:T(8,128)S(1)}, f32[8,512]{1,0:T(8,128)S(1)}, u32[]{:S(2)}, u32[]{:S(2)}) collective-permute-start(f32[8,512]{1,0:T(8,128)S(1)} %add_add_fusion.1), channel_id=1, source_target_pairs={{0,12},{1,13},{2,14},{3,15},{4,8},{5,9},{6,10},{7,11},{8,4},{9,5},... | collective-permute-start | bytes 49160 | tf_op jit(solution)/shard_map/ppermute | solution.py:65
  73.4 6.3 %collective-permute-start.11 = (f32[8,512]{1,0:T(8,128)S(1)}, f32[8,512]{1,0:T(8,128)S(1)}, u32[]{:S(2)}, u32[]{:S(2)}) collective-permute-start(f32[8,512]{1,0:T(8,128)S(1)} %add_add_fusion.1), channel_id=1, source_target_pairs={{0,4},{1,5},{2,6},{3,7},{4,0},{5,1},{6,2},{7,3},{8,12},{9,13},{10,... | collective-permute-start | bytes 49160 | tf_op jit(solution)/shard_map/ppermute | solution.py:65
  74.9 5.7 %copy-start.2 = (f32[256,1024]{1,0:T(8,128)S(1)}, f32[256,1024]{1,0:T(8,128)}, u32[]{:S(2)}) copy-start(f32[256,1024]{1,0:T(8,128)} %get-tuple-element.18) | copy-start | bytes 3145732

commit v2 on v1

v2 whole, which is shorter than its diff:
```python
import functools
import math

import jax
import jax.numpy as jnp
from jax import lax
from jax.experimental import pallas as pl
from jax.experimental.pallas import tpu as pltpu
from jax.sharding import PartitionSpec as P


SEG_LEN = 64
AXES = ("sp", "tp")
LOG2E = math.log2(math.e)
MASKED = -1e30
F32 = jnp.float32
BF16 = jnp.bfloat16
NT = (((1,), (1,)), ((), ()))
NN = (((1,), (0,)), ((), ()))


def shifted(block, distance):
    count = lax.axis_size(AXES)
    route = [(i - distance, i) for i in range(count) if 0 <= i - distance < count]
    return lax.ppermute(block, AXES, route)


def prime_radices(count):
    radices = []
    twos = 0
    while count % 2 == 0:
        count //= 2
        twos += 1
    while twos > 0:
        take = 2 if twos != 3 else 3
        take = min(take, twos)
        radices.append(2**take)
        twos -= take
    factor = 3
    while count > 1:
        while count % factor == 0:
            radices.append(factor)
            count //= factor
        factor += 2
    return radices


def pair_tree(parts):
    while len(parts) > 1:
        parts = [parts[i] + parts[i + 1] for i in range(0, len(parts), 2)]
    return parts[0]


def all_sum(part):
    count = lax.axis_size(AXES)
    me = lax.axis_index(AXES)
    stride = 1
    for radix in prime_radices(count):
        if radix & (radix - 1) == 0:
            parts = [part]
            for step in range(1, radix):
                route = [(i, i ^ (step * stride)) for i in range(count)]
                parts.append(lax.ppermute(part, AXES, route))
            part = pair_tree(parts)
        else:
            digit = (me // stride) % radix
            parts = [part]
            for step in range(1, radix):
                route = []
                for i in range(count):
                    d = (i // stride) % radix
                    route.append((i, i + (((d - step) % radix) - d) * stride))
                parts.append(lax.ppermute(part, AXES, route))
            total = jnp.zeros_like(part)
            for d in range(radix):
                value = parts[0]
                for step in range(1, radix):
                    value = jnp.where((digit + step) % radix == d, parts[step], value)
                total = total + value
            part = total
        stride *= radix
    return part


def prep_tiles(head_count, table_ref, chunk_ref, tile_ref):
    size = tile_ref.shape[2]
    table_len = table_ref.shape[1]
    span = chunk_ref.shape[1]
    pad = size - (SEG_LEN - 1)
    lane = lax.broadcasted_iota(jnp.int32, (head_count, span), 1)
    table = table_ref[...] * LOG2E
    first, last = table[:, :1], table[:, table_len - 1 :]
    wide = jnp.concatenate([table, jnp.zeros((head_count, span - table_len), F32)], axis=1)
    moved = pltpu.roll(wide, pad, 1)
    moved = jnp.where(lane < pad, first, jnp.where(lane >= pad + table_len, last, moved))
    chunk_ref[...] = moved
    row = lax.broadcasted_iota(jnp.int32, (size, size), 0)
    col = lax.broadcasted_iota(jnp.int32, (size, size), 1)

    @pl.loop(0, head_count)
    def _(head):
        rolled = []
        lines = chunk_ref[pl.ds(head, 1), :]
        for c in range(4):
            line = jnp.broadcast_to(lines[:, c * size : (c + 1) * size], (size, size))
            rolled.append(pltpu.roll(line, 0, 1, stride=1, stride_axis=0))
        for b in range(3):
            tile = jnp.where(col >= row, rolled[b + 1], rolled[b])
            if b == 0:
                tile = jnp.where((row // SEG_LEN) <= (col // SEG_LEN), tile, MASKED)
            tile_ref[head, b] = tile


def unroll_sum(tile):
    size = tile.shape[0]
    group = 8
    parts = []
    for start in range(0, size, group):
        part = tile[start : start + group, :]
        parts.append(part if start == 0 else pltpu.roll(part, size - start, 1))
    total = pair_tree(parts)
    row = lax.broadcasted_iota(jnp.int32, total.shape, 0)
    for bit in (1, 2, 4):
        total = jnp.where((row & bit) != 0, pltpu.roll(total, size - bit, 1), total)
    return jnp.sum(total, axis=0, keepdims=True)


def score_terms(lag, key, value, query, grad, log_row, dot_row, tiles, const, inv_root):
    rows = key.shape[0]
    half = rows // 2
    raw = lax.dot_general(key, query, NT, preferred_element_type=F32)
    wgt = lax.dot_general(value, grad, NT, preferred_element_type=F32)
    row = lax.broadcasted_iota(jnp.int32, (half, half), 0) // SEG_LEN
    col = lax.broadcasted_iota(jnp.int32, (half, half), 1) // SEG_LEN
    acc = [None, None, None, None]
    w_rows, s_rows = [], []
    for r in range(2):
        w_cols, s_cols = [], []
        for c in range(2):
            if (lag == 0 and r > c) or (lag == 2 and c > r):
                w_cols.append(jnp.zeros((half, half), BF16))
                s_cols.append(jnp.zeros((half, half), BF16))
                continue
            rs, cs = slice(r * half, (r + 1) * half), slice(c * half, (c + 1) * half)
            level = min(2 * lag + c - r, 3)
            lrow = log_row[:, cs]
            bias = const - lrow if level == 3 else tiles[level] - lrow
            weight = jnp.exp2(raw[rs, cs] * (inv_root * LOG2E) + bias)
            if lag == 2 and r == c:
                weight = jnp.where(col <= row, weight, 0.0)
            score = weight * (wgt[rs, cs] - dot_row[:, cs])
            acc[level] = score if acc[level] is None else acc[level] + score
            w_cols.append(weight.astype(BF16))
            s_cols.append(score.astype(BF16))
        w_rows.append(jnp.concatenate(w_cols, axis=1))
        s_rows.append(jnp.concatenate(s_cols, axis=1))
    return jnp.concatenate(w_rows, axis=0), jnp.concatenate(s_rows, axis=0), acc


def table_lines(acc, size):
    row = lax.broadcasted_iota(jnp.int32, (size, size), 0)
    col = lax.broadcasted_iota(jnp.int32, (size, size), 1)
    zero = jnp.zeros((size, size), F32)
    lines = []
    for c in range(4):
        upper = acc[c - 1] if c > 0 else None
        lower = acc[c] if c < 3 else None
        line = None
        if upper is not None or lower is not None:
            mixed = jnp.where(
                col >= row,
                zero if upper is None else upper,
                zero if lower is None else lower,
            )
            line = unroll_sum(mixed)
        if c == 3 and acc[3] is not None:
            extra = jnp.sum(acc[3], axis=0, keepdims=True)
            line = extra if line is None else line + extra
        lines.append(line)
    return lines


def lag_kernel(lag, heads_step, head_count, *refs):
    if lag == 0:
        (k_ref, v_ref, q_ref, g_ref, st_ref, table_ref,
         dq_ref, dk_ref, dv_ref, tab_ref, kt_ref, tile_ref, chunk_ref) = refs
        prep_tiles(head_count, table_ref, chunk_ref, tile_ref)
    elif lag == 2:
        (k_ref, v_ref, q_ref, g_ref, st_ref, kt_ref, tile_ref, chunk_ref, dk_in, dv_in, tab_in,
         dq_ref, dk_ref, dv_ref, tab_ref) = refs
    else:
        (k_ref, v_ref, q_ref, g_ref, st_ref, kt_ref, tile_ref, chunk_ref, tab_in,
         dq_ref, tab_ref, w_ref, s_ref) = refs
    size = tile_ref.shape[2]
    head_dim = k_ref.shape[1] // head_count
    inv_root = head_dim ** (-0.5)

    @pl.loop(0, head_count // heads_step)
    def _(step):
        for i in range(heads_step):
            head = step * heads_step + i
            cols = pl.ds(pl.multiple_of(head * head_dim, head_dim), head_dim)
            key, value, query, grad = k_ref[:, cols], v_ref[:, cols], q_ref[:, cols], g_ref[:, cols]
            log_row = st_ref[pl.ds(head, 1), :]
            dot_row = st_ref[pl.ds(head + head_count, 1), :]
            const = chunk_ref[pl.ds(head, 1), :][:, 3 * size :]
            tiles = [None if lag == 2 else tile_ref[head, b] for b in range(3)]
            weights, scores, acc = score_terms(
                lag, key, value, query, grad, log_row, dot_row, tiles, const, inv_root
            )
            if lag == 0:
                turned = key.T
                kt_ref[cols, :] = turned
            else:
                turned = kt_ref[cols, :]
            dq = lax.dot_general(turned, scores, NN, preferred_element_type=F32) * inv_root
            dq_ref[cols, :] = dq.astype(dq_ref.dtype)
            lines = [
                jnp.zeros((1, size), F32) if line is None else line
                for line in table_lines(acc, size)
            ]
            lines = jnp.concatenate(lines, axis=1)
            row_at = pl.ds(head, 1)
            tab_ref[row_at, :] = lines if lag == 0 else tab_in[row_at, :] + lines
            if lag == 1:
                w_ref[head] = weights
                s_ref[head] = scores
            else:
                dk = lax.dot_general(scores, query, NN, preferred_element_type=F32)
                dv = lax.dot_general(weights, grad, NN, preferred_element_type=F32)
                dk_ref[:, cols] = dk if lag == 0 else dk + dk_in[:, cols]
                dv_ref[:, cols] = dv if lag == 0 else dv + dv_in[:, cols]


def close_kernel(heads_step, w_ref, s_ref, q_ref, g_ref, dk_in, dv_in, dk_ref, dv_ref):
    head_count = w_ref.shape[0]
    head_dim = q_ref.shape[1] // head_count
    inv_root = head_dim ** (-0.5)

    @pl.loop(0, head_count // heads_step)
    def _(step):
        for i in range(heads_step):
            head = step * heads_step + i
            cols = pl.ds(pl.multiple_of(head * head_dim, head_dim), head_dim)
            dk = lax.dot_general(s_ref[head], q_ref[:, cols], NN, preferred_element_type=F32)
            dv = lax.dot_general(w_ref[head], g_ref[:, cols], NN, preferred_element_type=F32)
            dk_ref[:, cols] = ((dk + dk_in[:, cols]) * inv_root).astype(BF16)
            dv_ref[:, cols] = (dv + dv_in[:, cols]).astype(BF16)


def query_kernel(heads_step, head_count, dq_ref, one_ref, two_ref, out_ref):
    head_dim = dq_ref.shape[0] // head_count

    @pl.loop(0, head_count // heads_step)
    def _(step):
        for i in range(heads_step):
            cols = pl.ds(pl.multiple_of((step * heads_step + i) * head_dim, head_dim), head_dim)
            total = dq_ref[cols, :] + one_ref[cols, :].astype(F32) + two_ref[cols, :].astype(F32)
            out_ref[:, cols] = total.T.astype(BF16)


def local(query_rows, key_rows, value_rows, out_grad, log_totals, out_dot, bias_table):
    rows, feats = query_rows.shape
    heads = log_totals.shape[1]
    table_len = bias_table.shape[1]
    half = rows // 2
    pair_flops = 2 * rows * rows * feats

    def cost(matmuls):
        return pl.CostEstimate(
            flops=matmuls * pair_flops,
            bytes_accessed=8 * rows * feats,
            transcendentals=heads * rows * rows,
        )

    def call(body, matmuls, outs, *args):
        return pl.pallas_call(
            body,
            in_specs=[pl.BlockSpec(memory_space=pltpu.VMEM)] * len(args),
            out_specs=[pl.BlockSpec(memory_space=pltpu.VMEM)] * len(outs),
            out_shape=outs,
            cost_estimate=cost(matmuls),
            compiler_params=pltpu.CompilerParams(vmem_limit_bytes=16 * 2**20),
        )(*args)

    moved = {}
    stats = jnp.concatenate([log_totals * LOG2E, out_dot], axis=1).T
    for lag in (1, 2):
        parts = []
        for part in (query_rows, out_grad, stats):
            parts.append(shifted(part, -lag))
        moved[lag] = parts

    rows_f32 = pltpu.VMEM((rows, feats), F32)
    rows_b16 = pltpu.VMEM((rows, feats), BF16)
    turn_f32 = pltpu.VMEM((feats, rows), F32)
    turn_b16 = pltpu.VMEM((feats, rows), BF16)
    tab_shape = pltpu.VMEM((heads, 4 * half), F32)
    sq_shape = pltpu.VMEM((heads, rows, rows), BF16)
    tile_shape = pltpu.VMEM((heads, 3, half, half), F32)

    body = functools.partial
    dq0, dk, dv, tab, turned, tiles, chunks = call(
        body(lag_kernel, 0, 2, heads), 5,
        [turn_f32, rows_f32, rows_f32, tab_shape, turn_b16, tile_shape, tab_shape],
        key_rows, value_rows, query_rows, out_grad, stats, bias_table,
    )
    dq2, dk, dv, tab = call(
        body(lag_kernel, 2, 2, heads), 5,
        [turn_b16, rows_f32, rows_f32, tab_shape],
        key_rows, value_rows, *moved[2], turned, tiles, chunks, dk, dv, tab,
    )
    back2 = shifted(dq2, 2)
    dq1, tab, weights, scores = call(
        body(lag_kernel, 1, 2, heads), 3,
        [turn_b16, tab_shape, sq_shape, sq_shape],
        key_rows, value_rows, *moved[1], turned, tiles, chunks, tab,
    )
    back1 = shifted(dq1, 1)
    lines = all_sum(tab)
    out_shape = jax.ShapeDtypeStruct((rows, feats), BF16)
    grad_key, grad_value = call(
        body(close_kernel, 2), 2, [out_shape, out_shape],
        weights, scores, moved[1][0], moved[1][1], dk, dv,
    )
    grad_query, = call(body(query_kernel, 2, heads), 1, [out_shape], dq0, back1, back2)
    start = half - (SEG_LEN - 1)
    grad_table = jnp.concatenate(
        [
            lines[:, start : start + table_len - 1],
            jnp.sum(lines[:, start + table_len - 1 :], axis=1, keepdims=True),
        ],
        axis=1,
    )
    return grad_query, grad_key, grad_value, grad_table


def solution(mesh):
    placed = (P(AXES, None),) * 6 + (P(),)
    return jax.shard_map(
        local,
        mesh=mesh,
        in_specs=placed,
        out_specs=(P(AXES, None),) * 3 + (P(),),
        check_vma=False,
    )
```

time: 82.7 us -> 73.4 us (0.89)
  the two profiles are of different devices: /device:TPU:3 before, /device:TPU:0 now
where the time goes in v2:
time: 73.4 us; the launch traced here: 72.8 us
  starting transfers between devices  38.9 us (53%)
  Pallas kernels  14.4 us (20%)
  waiting for transfers between devices  11.4 us (16%)
  local copies, waits for them, and re-layouts  5.02 us (7%)
  other arithmetic  2.21 us (3%)
  between operations  0.8 us (1%)
    ppermute x10, starting transfers between devices, all_sum(): parts.append(lax.ppermute(part, AXES, route))  25.3 us
    pallas_call x5, Pallas kernels, call(): pl.pallas_call(body, in_specs=[pl.BlockSpec(memory_space=pltpu.VMEM)] * l...  14.4 us
    ppermute x8, starting transfers between devices, shifted(): return lax.ppermute(block, AXES, route)  13.6 us
    ppermute x8, waiting for transfers between devices, shifted(): return lax.ppermute(block, AXES, route)  9.28 us
    unnamed x10, local copies, waits for them, and re-layouts  4.87 us
    ppermute x10, waiting for transfers between devices, all_sum(): parts.append(lax.ppermute(part, AXES, route))  2.15 us
  transfers between devices with their start and end apart: 18, of which 3 were waited for; matrix products, arithmetic and copies ran while one was open for 3% of the time, Pallas kernels for 14%

profile of v2, /device:TPU:0, one launch (start us, length us, event | category | flops | bytes accessed | tf_op | source)
XLA Modules:
  0.0 72.8 jit_solution(6079242078880447473)
XLA Ops:
  0.6 1.3 %collective-permute-start.3 = (bf16[256,1024]{1,0:T(8,128)(2,1)}, bf16[256,1024]{1,0:T(8,128)(2,1)S(1)}, u32[]{:S(2)}, u32[]{:S(2)}) collective-permute-start(bf16[256,1024]{1,0:T(8,128)(2,1)} %refs_2_.1), channel_id=1, source_target_pairs={{2,0},{3,1},{4,2},{5,3},{6,4},{7,5},{8,6},{9,7},{10,8},{11,9},{12,... | collective-permute-start | bytes 1572872 | tf_op jit(solution)/shard_map/ppermute | solution.py:25
  1.9 1.3 %collective-permute-start.4 = (bf16[256,1024]{1,0:T(8,128)(2,1)}, bf16[256,1024]{1,0:T(8,128)(2,1)S(1)}, u32[]{:S(2)}, u32[]{:S(2)}) collective-permute-start(bf16[256,1024]{1,0:T(8,128)(2,1)} %refs_3_.1), channel_id=1, source_target_pairs={{2,0},{3,1},{4,2},{5,3},{6,4},{7,5},{8,6},{9,7},{10,8},{11,9},{12,... | collective-permute-start | bytes 1572872 | tf_op jit(solution)/shard_map/ppermute | solution.py:25
  3.2 1.3 %collective-permute-start = (bf16[256,1024]{1,0:T(8,128)(2,1)}, bf16[256,1024]{1,0:T(8,128)(2,1)S(1)}, u32[]{:S(2)}, u32[]{:S(2)}) collective-permute-start(bf16[256,1024]{1,0:T(8,128)(2,1)} %refs_2_.1), channel_id=1, source_target_pairs={{1,0},{2,1},{3,2},{4,3},{5,4},{6,5},{7,6},{8,7},{9,8},{10,9},{11,1... | collective-permute-start | bytes 1572872 | tf_op jit(solution)/shard_map/ppermute | solution.py:25
  4.5 1.3 %collective-permute-start.1 = (bf16[256,1024]{1,0:T(8,128)(2,1)}, bf16[256,1024]{1,0:T(8,128)(2,1)S(1)}, u32[]{:S(2)}, u32[]{:S(2)}) collective-permute-start(bf16[256,1024]{1,0:T(8,128)(2,1)} %refs_3_.1), channel_id=1, source_target_pairs={{1,0},{2,1},{3,2},{4,3},{5,4},{6,5},{7,6},{8,7},{9,8},{10,9},{11,1... | collective-permute-start | bytes 1572872 | tf_op jit(solution)/shard_map/ppermute | solution.py:25
  5.8 0.7 broadcast_multiply_fusion
  6.5 0.7 maximum_bitcast_fusion.refs_4_
  7.2 1.3 %collective-permute-start.5 = (f32[16,256]{1,0:T(8,128)S(1)}, f32[16,256]{1,0:T(8,128)S(1)}, u32[]{:S(2)}, u32[]{:S(2)}) collective-permute-start(f32[16,256]{1,0:T(8,128)S(1)} %maximum_bitcast_fusion.refs_4_), channel_id=1, source_target_pairs={{2,0},{3,1},{4,2},{5,3},{6,4},{7,5},{8,6},{9,7},{10,8},{11,9},{12,... | collective-permute-start | bytes 49160 | tf_op jit(solution)/shard_map/ppermute | solution.py:25
  8.5 1.0 %copy-done = bf16[256,1024]{1,0:T(8,128)(2,1)S(1)} copy-done((bf16[256,1024]{1,0:T(8,128)(2,1)S(1)}, bf16[256,1024]{1,0:T(8,128)(2,1)}, u32[]{:S(2)}) %copy-start) | copy-done | bytes 524312
  9.6 1.0 %copy-done.1 = bf16[256,1024]{1,0:T(8,128)(2,1)S(1)} copy-done((bf16[256,1024]{1,0:T(8,128)(2,1)S(1)}, bf16[256,1024]{1,0:T(8,128)(2,1)}, u32[]{:S(2)}) %copy-start.1) | copy-done | bytes 524312
  10.6 1.0 %copy-done.2 = bf16[256,1024]{1,0:T(8,128)(2,1)S(1)} copy-done((bf16[256,1024]{1,0:T(8,128)(2,1)S(1)}, bf16[256,1024]{1,0:T(8,128)(2,1)}, u32[]{:S(2)}) %copy-start.2) | copy-done | bytes 524312
  11.6 1.0 %copy-done.3 = bf16[256,1024]{1,0:T(8,128)(2,1)S(1)} copy-done((bf16[256,1024]{1,0:T(8,128)(2,1)S(1)}, bf16[256,1024]{1,0:T(8,128)(2,1)}, u32[]{:S(2)}) %copy-start.3) | copy-done | bytes 524312
  12.7 0.7 copy-done.4
  13.4 4.6 %shard_map.102 = (f32[1024,256]{1,0:T(8,128)S(1)}, f32[256,1024]{1,0:T(8,128)S(1)}, f32[256,1024]{1,0:T(8,128)S(1)}, f32[8,512]{1,0:T(8,128)S(1)}, bf16[1024,256...) custom-call(bf16[256,1024]{1,0:T(8,128)(2,1)S(1)} %copy-done, ...), custom_call_target="tpu_custom_call" | custom-call | flops 671088640 | bytes 2097152 | tf_op jit(solution)/shard_map/pallas_call | solution.py:277
  18.0 1.3 %collective-permute-start.2 = (f32[16,256]{1,0:T(8,128)S(1)}, f32[16,256]{1,0:T(8,128)S(1)}, u32[]{:S(2)}, u32[]{:S(2)}) collective-permute-start(f32[16,256]{1,0:T(8,128)S(1)} %maximum_bitcast_fusion.refs_4_), channel_id=1, source_target_pairs={{1,0},{2,1},{3,2},{4,3},{5,4},{6,5},{7,6},{8,7},{9,8},{10,9},{11,1... | collective-permute-start | bytes 49160 | tf_op jit(solution)/shard_map/ppermute | solution.py:25
  19.3 3.0 %shard_map.103 = (bf16[1024,256]{1,0:T(8,128)(2,1)S(1)}, f32[256,1024]{1,0:T(8,128)S(1)}, f32[256,1024]{1,0:T(8,128)S(1)}, f32[8,512]{1,0:T(8,128)S(1)}) custom-call(bf16[256,1024]{1,0:T(8,128)(2,1)S(1)} %copy-done, bf16[256,1024]{1,0:T(8,128)(2,1)S(1)} %copy-done.1, bf16[256,1024]{1,0:T(8,128)(2,1)S(1)} %collective-permute-done.3.refs_2_, ...), custom_call_target="tpu_custom_call" | custom-call | flops 671088640 | bytes 2097152 | tf_op jit(solution)/shard_map/pallas_call | solution.py:277
  22.3 9.3 %collective-permute-done.2.refs_4_ = f32[16,256]{1,0:T(8,128)S(1)} collective-permute-done((f32[16,256]{1,0:T(8,128)S(1)}, f32[16,256]{1,0:T(8,128)S(1)}, u32[]{:S(2)}, u32[]{:S(2)}) %collective-permute-start.2) | collective-permute-done | bytes 16416 | tf_op jit(solution)/shard_map/ppermute | solution.py:25
  31.6 3.3 %shard_map.104 = (bf16[1024,256]{1,0:T(8,128)(2,1)S(1)}, f32[8,512]{1,0:T(8,128)S(1)}, bf16[8,256,256]{2,1,0:T(8,128)(2,1)S(1)}, bf16[8,256,256]{2,1,0:T(8,128)(2,1)S(1)}) custom-call(bf16[256,1024]{1,0:T(8,128)(2,1)S(1)} %copy-done, bf16[256,1024]{1,0:T(8,128)(2,1)S(1)} %copy-done.1, bf16[256,1024]{1,0:T(8,128)(2,1)S(1)} %collective-permute-done.refs_2_.q_ref, ...), custom_call_target="tpu_custom_call" | custom-call | flops 402653184 | bytes 2097152 | tf_op jit(solution)/shard_map/pallas_call | solution.py:277
  34.9 4.8 %collective-permute-start.10 = (f32[8,512]{1,0:T(8,128)S(1)}, f32[8,512]{1,0:T(8,128)S(1)}, u32[]{:S(2)}, u32[]{:S(2)}) collective-permute-start(f32[8,512]{1,0:T(8,128)S(1)} %get-tuple-element.37), channel_id=1, source_target_pairs={{0,3},{1,2},{2,1},{3,0},{4,7},{5,6},{6,5},{7,4},{8,11},{9,10},{10,... | collective-permute-start | bytes 49160 | tf_op jit(solution)/shard_map/ppermute | solution.py:63
  39.7 0.2 collective-permute-start.9
  39.9 3.8 %collective-permute-start.6 = (bf16[1024,256]{1,0:T(8,128)(2,1)S(1)}, bf16[1024,256]{1,0:T(8,128)(2,1)S(1)}, u32[]{:S(2)}, u32[]{:S(2)}) collective-permute-start(bf16[1024,256]{1,0:T(8,128)(2,1)S(1)} %get-tuple-element.29), channel_id=1, source_target_pairs={{0,1},{1,2},{2,3},{3,4},{4,5},{5,6},{6,7},{7,8},{8,9},{9,10},{10,1... | collective-permute-start | bytes 1572872 | tf_op jit(solution)/shard_map/ppermute | solution.py:25
  43.6 2.1 %collective-permute-start.7 = (bf16[1024,256]{1,0:T(8,128)(2,1)S(1)}, bf16[1024,256]{1,0:T(8,128)(2,1)S(1)}, u32[]{:S(2)}, u32[]{:S(2)}) collective-permute-start(bf16[1024,256]{1,0:T(8,128)(2,1)S(1)} %get-tuple-element.30), channel_id=1, source_target_pairs={{0,2},{1,3},{2,4},{3,5},{4,6},{5,7},{6,8},{7,9},{8,10},{9,11},{10,... | collective-permute-start | bytes 1572872 | tf_op jit(solution)/shard_map/ppermute | solution.py:25
  45.8 2.3 %collective-permute-start.11 = (f32[8,512]{1,0:T(8,128)S(1)}, f32[8,512]{1,0:T(8,128)S(1)}, u32[]{:S(2)}, u32[]{:S(2)}) collective-permute-start(f32[8,512]{1,0:T(8,128)S(1)} %add_add_fusion.1), channel_id=1, source_target_pairs={{0,4},{1,5},{2,6},{3,7},{4,0},{5,1},{6,2},{7,3},{8,12},{9,13},{10,... | collective-permute-start | bytes 49160 | tf_op jit(solution)/shard_map/ppermute | solution.py:63
  48.1 1.6 %collective-permute-start.12 = (f32[8,512]{1,0:T(8,128)S(1)}, f32[8,512]{1,0:T(8,128)S(1)}, u32[]{:S(2)}, u32[]{:S(2)}) collective-permute-start(f32[8,512]{1,0:T(8,128)S(1)} %add_add_fusion.1), channel_id=1, source_target_pairs={{0,8},{1,9},{2,10},{3,11},{4,12},{5,13},{6,14},{7,15},{8,0},{9,1},... | collective-permute-start | bytes 49160 | tf_op jit(solution)/shard_map/ppermute | solution.py:63
  49.7 0.1 collective-permute-done.11
  49.8 11.7 %collective-permute-start.14 = (f32[8,512]{1,0:T(8,128)S(1)}, f32[8,512]{1,0:T(8,128)S(1)}, u32[]{:S(2)}, u32[]{:S(2)}) collective-permute-start(f32[8,512]{1,0:T(8,128)S(1)} %add_add_fusion.1), channel_id=1, source_target_pairs={{0,16},{1,17},{2,18},{3,19},{4,20},{5,21},{6,22},{7,23},{8,24},{9,... | collective-permute-start | bytes 49160 | tf_op jit(solution)/shard_map/ppermute | solution.py:63
  61.5 2.6 %collective-permute-start.16 = (f32[8,512]{1,0:T(8,128)S(1)}, f32[8,512]{1,0:T(8,128)S(1)}, u32[]{:S(2)}, u32[]{:S(2)}) collective-permute-start(f32[8,512]{1,0:T(8,128)S(1)} %add_add_fusion.1), channel_id=1, source_target_pairs={{0,24},{1,25},{2,26},{3,27},{4,28},{5,29},{6,30},{7,31},{8,16},{9,... | collective-permute-start | bytes 49160 | tf_op jit(solution)/shard_map/ppermute | solution.py:63
  64.1 2.2 %collective-permute-start.17 = (f32[8,512]{1,0:T(8,128)S(1)}, f32[8,512]{1,0:T(8,128)S(1)}, u32[]{:S(2)}, u32[]{:S(2)}) collective-permute-start(f32[8,512]{1,0:T(8,128)S(1)} %add_add_fusion.1), channel_id=1, source_target_pairs={{0,28},{1,29},{2,30},{3,31},{4,24},{5,25},{6,26},{7,27},{8,20},{9,... | collective-permute-start | bytes 49160 | tf_op jit(solution)/shard_map/ppermute | solution.py:63
  66.3 2.3 %shard_map.106 = (bf16[256,1024]{1,0:T(8,128)(2,1)}, bf16[256,1024]{1,0:T(8,128)(2,1)}) custom-call(bf16[8,256,256]{2,1,0:T(8,128)(2,1)S(1)} %get-tuple-element.31.w_ref, bf16[8,256,256]{2,1,0:T(8,128)(2,1)S(1)} %get-tuple-element.32.s_ref, bf16[256,1024]{1,0:T(8,128)(2,1)S(1)} %collective-permute-done.refs_2_.q_ref, ...), custom_call_target="tpu_custom_call" | custom-call | flops 268435456 | bytes 2097152 | tf_op jit(solution)/shard_map/pallas_call | solution.py:277
  68.5 2.0 %collective-permute-done.17 = f32[8,512]{1,0:T(8,128)S(1)} collective-permute-done((f32[8,512]{1,0:T(8,128)S(1)}, f32[8,512]{1,0:T(8,128)S(1)}, u32[]{:S(2)}, u32[]{:S(2)}) %collective-permute-start.17) | collective-permute-done | bytes 16416 | tf_op jit(solution)/shard_map/ppermute | solution.py:63
  70.6 0.1 slice_reduce_fusion
  70.8 0.7 pad_maximum_fusion
  71.5 1.3 %shard_map.105 = bf16[256,1024]{1,0:T(8,128)(2,1)} custom-call(f32[1024,256]{1,0:T(8,128)S(1)} %get-tuple-element.21.dq_ref, bf16[1024,256]{1,0:T(8,128)(2,1)S(1)} %collective-permute-done.6.one_ref, bf16[1024,256]{1,0:T(8,128)(2,1)S(1)} %collective-permute-done.7.two_ref), custom_call_target="tpu_custom_call" | custom-call | flops 134217728 | bytes 2097152 | tf_op jit(solution)/shard_map/pallas_call | solution.py:277
  (27 shorter events, 0.2 us)
Async XLA Ops:
  0.6 18.7 %collective-permute-start.3 = (bf16[256,1024]{1,0:T(8,128)(2,1)}, bf16[256,1024]{1,0:T(8,128)(2,1)S(1)}, u32[]{:S(2)}, u32[]{:S(2)}) collective-permute-start(bf16[256,1024]{1,0:T(8,128)(2,1)} %refs_2_.1), channel_id=1, source_target_pairs={{2,0},{3,1},{4,2},{5,3},{6,4},{7,5},{8,6},{9,7},{10,8},{11,9},{12,... | collective-permute-start | bytes 1572872 | tf_op jit(solution)/shard_map/ppermute | solution.py:25
  1.9 17.4 %collective-permute-start.4 = (bf16[256,1024]{1,0:T(8,128)(2,1)}, bf16[256,1024]{1,0:T(8,128)(2,1)S(1)}, u32[]{:S(2)}, u32[]{:S(2)}) collective-permute-start(bf16[256,1024]{1,0:T(8,128)(2,1)} %refs_3_.1), channel_id=1, source_target_pairs={{2,0},{3,1},{4,2},{5,3},{6,4},{7,5},{8,6},{9,7},{10,8},{11,9},{12,... | collective-permute-start | bytes 1572872 | tf_op jit(solution)/shard_map/ppermute | solution.py:25
  3.2 28.4 %collective-permute-start = (bf16[256,1024]{1,0:T(8,128)(2,1)}, bf16[256,1024]{1,0:T(8,128)(2,1)S(1)}, u32[]{:S(2)}, u32[]{:S(2)}) collective-permute-start(bf16[256,1024]{1,0:T(8,128)(2,1)} %refs_2_.1), channel_id=1, source_target_pairs={{1,0},{2,1},{3,2},{4,3},{5,4},{6,5},{7,6},{8,7},{9,8},{10,9},{11,1... | collective-permute-start | bytes 1572872 | tf_op jit(solution)/shard_map/ppermute | solution.py:25
  4.5 27.1 %collective-permute-start.1 = (bf16[256,1024]{1,0:T(8,128)(2,1)}, bf16[256,1024]{1,0:T(8,128)(2,1)S(1)}, u32[]{:S(2)}, u32[]{:S(2)}) collective-permute-start(bf16[256,1024]{1,0:T(8,128)(2,1)} %refs_3_.1), channel_id=1, source_target_pairs={{1,0},{2,1},{3,2},{4,3},{5,4},{6,5},{7,6},{8,7},{9,8},{10,9},{11,1... | collective-permute-start | bytes 1572872 | tf_op jit(solution)/shard_map/ppermute | solution.py:25
  7.2 10.8 %collective-permute-start.5 = (f32[16,256]{1,0:T(8,128)S(1)}, f32[16,256]{1,0:T(8,128)S(1)}, u32[]{:S(2)}, u32[]{:S(2)}) collective-permute-start(f32[16,256]{1,0:T(8,128)S(1)} %maximum_bitcast_fusion.refs_4_), channel_id=1, source_target_pairs={{2,0},{3,1},{4,2},{5,3},{6,4},{7,5},{8,6},{9,7},{10,8},{11,9},{12,... | collective-permute-start | bytes 49160 | tf_op jit(solution)/shard_map/ppermute | solution.py:25
  8.5 1.0 %copy-start = (bf16[256,1024]{1,0:T(8,128)(2,1)S(1)}, bf16[256,1024]{1,0:T(8,128)(2,1)}, u32[]{:S(2)}) copy-start(bf16[256,1024]{1,0:T(8,128)(2,1)} %refs_0_.5) | copy-start | bytes 1572868
  9.6 1.0 %copy-start.1 = (bf16[256,1024]{1,0:T(8,128)(2,1)S(1)}, bf16[256,1024]{1,0:T(8,128)(2,1)}, u32[]{:S(2)}) copy-start(bf16[256,1024]{1,0:T(8,128)(2,1)} %refs_1_.5) | copy-start | bytes 1572868
  10.6 1.0 %copy-start.2 = (bf16[256,1024]{1,0:T(8,128)(2,1)S(1)}, bf16[256,1024]{1,0:T(8,128)(2,1)}, u32[]{:S(2)}) copy-start(bf16[256,1024]{1,0:T(8,128)(2,1)} %refs_2_.1) | copy-start | bytes 1572868
  11.6 1.0 %copy-start.3 = (bf16[256,1024]{1,0:T(8,128)(2,1)S(1)}, bf16[256,1024]{1,0:T(8,128)(2,1)}, u32[]{:S(2)}) copy-start(bf16[256,1024]{1,0:T(8,128)(2,1)} %refs_3_.1) | copy-start | bytes 1572868
  12.7 0.7 copy-start.4
  18.0 13.6 %collective-permute-start.2 = (f32[16,256]{1,0:T(8,128)S(1)}, f32[16,256]{1,0:T(8,128)S(1)}, u32[]{:S(2)}, u32[]{:S(2)}) collective-permute-start(f32[16,256]{1,0:T(8,128)S(1)} %maximum_bitcast_fusion.refs_4_), channel_id=1, source_target_pairs={{1,0},{2,1},{3,2},{4,3},{5,4},{6,5},{7,6},{8,7},{9,8},{10,9},{11,1... | collective-permute-start | bytes 49160 | tf_op jit(solution)/shard_map/ppermute | solution.py:25
  34.9 10.9 %collective-permute-start.10 = (f32[8,512]{1,0:T(8,128)S(1)}, f32[8,512]{1,0:T(8,128)S(1)}, u32[]{:S(2)}, u32[]{:S(2)}) collective-permute-start(f32[8,512]{1,0:T(8,128)S(1)} %get-tuple-element.37), channel_id=1, source_target_pairs={{0,3},{1,2},{2,1},{3,0},{4,7},{5,6},{6,5},{7,4},{8,11},{9,10},{10,... | collective-permute-start | bytes 49160 | tf_op jit(solution)/shard_map/ppermute | solution.py:63
  39.7 6.1 %collective-permute-start.8 = (f32[8,512]{1,0:T(8,128)S(1)}, f32[8,512]{1,0:T(8,128)S(1)}, u32[]{:S(2)}, u32[]{:S(2)}) collective-permute-start(f32[8,512]{1,0:T(8,128)S(1)} %get-tuple-element.37), channel_id=1, source_target_pairs={{0,1},{1,0},{2,3},{3,2},{4,5},{5,4},{6,7},{7,6},{8,9},{9,8},{10,11... | collective-permute-start | bytes 49160 | tf_op jit(solution)/shard_map/ppermute | solution.py:63
  39.7 6.1 %collective-permute-start.9 = (f32[8,512]{1,0:T(8,128)S(1)}, f32[8,512]{1,0:T(8,128)S(1)}, u32[]{:S(2)}, u32[]{:S(2)}) collective-permute-start(f32[8,512]{1,0:T(8,128)S(1)} %get-tuple-element.37), channel_id=1, source_target_pairs={{0,2},{1,3},{2,0},{3,1},{4,6},{5,7},{6,4},{7,5},{8,10},{9,11},{10,... | collective-permute-start | bytes 49160 | tf_op jit(solution)/shard_map/ppermute | solution.py:63
  39.9 31.6 %collective-permute-start.6 = (bf16[1024,256]{1,0:T(8,128)(2,1)S(1)}, bf16[1024,256]{1,0:T(8,128)(2,1)S(1)}, u32[]{:S(2)}, u32[]{:S(2)}) collective-permute-start(bf16[1024,256]{1,0:T(8,128)(2,1)S(1)} %get-tuple-element.29), channel_id=1, source_target_pairs={{0,1},{1,2},{2,3},{3,4},{4,5},{5,6},{6,7},{7,8},{8,9},{9,10},{10,1... | collective-permute-start | bytes 1572872 | tf_op jit(solution)/shard_map/ppermute | solution.py:25
  43.6 27.9 %collective-permute-start.7 = (bf16[1024,256]{1,0:T(8,128)(2,1)S(1)}, bf16[1024,256]{1,0:T(8,128)(2,1)S(1)}, u32[]{:S(2)}, u32[]{:S(2)}) collective-permute-start(bf16[1024,256]{1,0:T(8,128)(2,1)S(1)} %get-tuple-element.30), channel_id=1, source_target_pairs={{0,2},{1,3},{2,4},{3,5},{4,6},{5,7},{6,8},{7,9},{8,10},{9,11},{10,... | collective-permute-start | bytes 1572872 | tf_op jit(solution)/shard_map/ppermute | solution.py:25
  45.8 4.0 %collective-permute-start.11 = (f32[8,512]{1,0:T(8,128)S(1)}, f32[8,512]{1,0:T(8,128)S(1)}, u32[]{:S(2)}, u32[]{:S(2)}) collective-permute-start(f32[8,512]{1,0:T(8,128)S(1)} %add_add_fusion.1), channel_id=1, source_target_pairs={{0,4},{1,5},{2,6},{3,7},{4,0},{5,1},{6,2},{7,3},{8,12},{9,13},{10,... | collective-permute-start | bytes 49160 | tf_op jit(solution)/shard_map/ppermute | solution.py:63
  48.1 13.4 %collective-permute-start.12 = (f32[8,512]{1,0:T(8,128)S(1)}, f32[8,512]{1,0:T(8,128)S(1)}, u32[]{:S(2)}, u32[]{:S(2)}) collective-permute-start(f32[8,512]{1,0:T(8,128)S(1)} %add_add_fusion.1), channel_id=1, source_target_pairs={{0,8},{1,9},{2,10},{3,11},{4,12},{5,13},{6,14},{7,15},{8,0},{9,1},... | collective-permute-start | bytes 49160 | tf_op jit(solution)/shard_map/ppermute | solution.py:63
  49.7 11.8 %collective-permute-start.13 = (f32[8,512]{1,0:T(8,128)S(1)}, f32[8,512]{1,0:T(8,128)S(1)}, u32[]{:S(2)}, u32[]{:S(2)}) collective-permute-start(f32[8,512]{1,0:T(8,128)S(1)} %add_add_fusion.1), channel_id=1, source_target_pairs={{0,12},{1,13},{2,14},{3,15},{4,8},{5,9},{6,10},{7,11},{8,4},{9,5},... | collective-permute-start | bytes 49160 | tf_op jit(solution)/shard_map/ppermute | solution.py:63
  49.8 14.3 %collective-permute-start.14 = (f32[8,512]{1,0:T(8,128)S(1)}, f32[8,512]{1,0:T(8,128)S(1)}, u32[]{:S(2)}, u32[]{:S(2)}) collective-permute-start(f32[8,512]{1,0:T(8,128)S(1)} %add_add_fusion.1), channel_id=1, source_target_pairs={{0,16},{1,17},{2,18},{3,19},{4,20},{5,21},{6,22},{7,23},{8,24},{9,... | collective-permute-start | bytes 49160 | tf_op jit(solution)/shard_map/ppermute | solution.py:63
  61.5 7.0 %collective-permute-start.15 = (f32[8,512]{1,0:T(8,128)S(1)}, f32[8,512]{1,0:T(8,128)S(1)}, u32[]{:S(2)}, u32[]{:S(2)}) collective-permute-start(f32[8,512]{1,0:T(8,128)S(1)} %add_add_fusion.1), channel_id=1, source_target_pairs={{0,20},{1,21},{2,22},{3,23},{4,16},{5,17},{6,18},{7,19},{8,28},{9,... | collective-permute-start | bytes 49160 | tf_op jit(solution)/shard_map/ppermute | solution.py:63
  61.5 7.0 %collective-permute-start.16 = (f32[8,512]{1,0:T(8,128)S(1)}, f32[8,512]{1,0:T(8,128)S(1)}, u32[]{:S(2)}, u32[]{:S(2)}) collective-permute-start(f32[8,512]{1,0:T(8,128)S(1)} %add_add_fusion.1), channel_id=1, source_target_pairs={{0,24},{1,25},{2,26},{3,27},{4,28},{5,29},{6,30},{7,31},{8,16},{9,... | collective-permute-start | bytes 49160 | tf_op jit(solution)/shard_map/ppermute | solution.py:63
  64.1 6.4 %collective-permute-start.17 = (f32[8,512]{1,0:T(8,128)S(1)}, f32[8,512]{1,0:T(8,128)S(1)}, u32[]{:S(2)}, u32[]{:S(2)}) collective-permute-start(f32[8,512]{1,0:T(8,128)S(1)} %add_add_fusion.1), channel_id=1, source_target_pairs={{0,28},{1,29},{2,30},{3,31},{4,24},{5,25},{6,26},{7,27},{8,20},{9,... | collective-permute-start | bytes 49160 | tf_op jit(solution)/shard_map/ppermute | solution.py:63

commit v3 on v2

--- a/solution.py
+++ b/solution.py
@@ -13,6 +13,7 @@
 AXES = ("sp", "tp")
 LOG2E = math.log2(math.e)
 MASKED = -1e30
+PACK = 128
 F32 = jnp.float32
 BF16 = jnp.bfloat16
 NT = (((1,), (1,)), ((), ()))
@@ -32,8 +33,7 @@
         count //= 2
         twos += 1
     while twos > 0:
-        take = 2 if twos != 3 else 3
-        take = min(take, twos)
+        take = 1 if not radices else min(2, twos)
         radices.append(2**take)
         twos -= take
     factor = 3
@@ -180,17 +180,44 @@
     return lines
 
 
+def read_stats(g_ref, stat_ref):
+    count = stat_ref.shape[0]
+    packed = g_ref[:, g_ref.shape[1] - PACK :].astype(F32).T
+    stat_ref[...] = packed[:count] + packed[count : 2 * count] + packed[2 * count : 3 * count]
+
+
+def fold_table(lines, table_len, size):
+    pad = size - (SEG_LEN - 1)
+    lane = lax.broadcasted_iota(jnp.int32, lines.shape, 1)
+    tail = jnp.sum(jnp.where(lane >= pad + table_len - 1, lines, 0.0), axis=1, keepdims=True)
+    moved = pltpu.roll(lines, lines.shape[1] - pad, 1)[:, :table_len]
+    lane = lax.broadcasted_iota(jnp.int32, moved.shape, 1)
+    return jnp.where(lane == table_len - 1, tail, moved)
+
+
 def lag_kernel(lag, heads_step, head_count, *refs):
+    copies = []
     if lag == 0:
-        (k_ref, v_ref, q_ref, g_ref, st_ref, table_ref,
-         dq_ref, dk_ref, dv_ref, tab_ref, kt_ref, tile_ref, chunk_ref) = refs
+        (k_hbm, v_hbm, q_hbm, g_ref, table_hbm,
+         dq_ref, dk_ref, dv_ref, tab_ref, kt_ref, tile_ref, chunk_ref, k_ref, v_ref,
+         q_ref, table_ref, stat_ref, sems) = refs
+        pairs = ((table_hbm, table_ref), (k_hbm, k_ref), (v_hbm, v_ref), (q_hbm, q_ref))
+        for i, (source, target) in enumerate(pairs):
+            copies.append(pltpu.make_async_copy(source, target, sems.at[i]))
+            copies[-1].start()
+        read_stats(g_ref, stat_ref)
+        copies[0].wait()
         prep_tiles(head_count, table_ref, chunk_ref, tile_ref)
+        for copy in copies[1:]:
+            copy.wait()
     elif lag == 2:
-        (k_ref, v_ref, q_ref, g_ref, st_ref, kt_ref, tile_ref, chunk_ref, dk_in, dv_in, tab_in,
-         dq_ref, dk_ref, dv_ref, tab_ref) = refs
+        (k_ref, v_ref, q_ref, g_ref, kt_ref, tile_ref, chunk_ref, dk_in, dv_in, tab_in,
+         dq_ref, dk_ref, dv_ref, tab_ref, stat_ref) = refs
+        read_stats(g_ref, stat_ref)
     else:
-        (k_ref, v_ref, q_ref, g_ref, st_ref, kt_ref, tile_ref, chunk_ref, tab_in,
-         dq_ref, tab_ref, w_ref, s_ref) = refs
+        (k_ref, v_ref, q_ref, g_ref, kt_ref, tile_ref, chunk_ref, tab_in,
+         dq_ref, out_tab_ref, w_ref, s_ref, tab_ref, stat_ref) = refs
+        read_stats(g_ref, stat_ref)
     size = tile_ref.shape[2]
     head_dim = k_ref.shape[1] // head_count
     inv_root = head_dim ** (-0.5)
@@ -201,8 +228,8 @@
             head = step * heads_step + i
             cols = pl.ds(pl.multiple_of(head * head_dim, head_dim), head_dim)
             key, value, query, grad = k_ref[:, cols], v_ref[:, cols], q_ref[:, cols], g_ref[:, cols]
-            log_row = st_ref[pl.ds(head, 1), :]
-            dot_row = st_ref[pl.ds(head + head_count, 1), :]
+            log_row = stat_ref[pl.ds(head, 1), :]
+            dot_row = stat_ref[pl.ds(head + head_count, 1), :]
             const = chunk_ref[pl.ds(head, 1), :][:, 3 * size :]
             tiles = [None if lag == 2 else tile_ref[head, b] for b in range(3)]
             weights, scores, acc = score_terms(
@@ -231,21 +258,22 @@
                 dk_ref[:, cols] = dk if lag == 0 else dk + dk_in[:, cols]
                 dv_ref[:, cols] = dv if lag == 0 else dv + dv_in[:, cols]
 
-
-def close_kernel(heads_step, w_ref, s_ref, q_ref, g_ref, dk_in, dv_in, dk_ref, dv_ref):
+    if lag == 1:
+        out_tab_ref[...] = fold_table(tab_ref[...], out_tab_ref.shape[1], size)
+
+
+def close_kernel(heads_step, scaled, w_ref, x_ref, part_ref, out_ref):
     head_count = w_ref.shape[0]
-    head_dim = q_ref.shape[1] // head_count
-    inv_root = head_dim ** (-0.5)
+    head_dim = out_ref.shape[1] // head_count
+    scale = head_dim ** (-0.5) if scaled else 1.0
 
     @pl.loop(0, head_count // heads_step)
     def _(step):
         for i in range(heads_step):
             head = step * heads_step + i
             cols = pl.ds(pl.multiple_of(head * head_dim, head_dim), head_dim)
-            dk = lax.dot_general(s_ref[head], q_ref[:, cols], NN, preferred_element_type=F32)
-            dv = lax.dot_general(w_ref[head], g_ref[:, cols], NN, preferred_element_type=F32)
-            dk_ref[:, cols] = ((dk + dk_in[:, cols]) * inv_root).astype(BF16)
-            dv_ref[:, cols] = (dv + dv_in[:, cols]).astype(BF16)
+            total = lax.dot_general(w_ref[head], x_ref[:, cols], NN, preferred_element_type=F32)
+            out_ref[:, cols] = ((total + part_ref[:, cols]) * scale).astype(BF16)
 
 
 def query_kernel(heads_step, head_count, dq_ref, one_ref, two_ref, out_ref):
@@ -259,12 +287,24 @@
             out_ref[:, cols] = total.T.astype(BF16)
 
 
+def packed_grads(out_grad, log_totals, out_dot):
+    stats = jnp.concatenate([log_totals * LOG2E, out_dot], axis=1)
+    high = lax.reduce_precision(stats, 8, 7)
+    rest = stats - high
+    mid = lax.reduce_precision(rest, 8, 7)
+    terms = jnp.concatenate([high, mid, rest - mid], axis=1).astype(BF16)
+    terms = jnp.pad(terms, ((0, 0), (0, PACK - terms.shape[1])))
+    return jnp.concatenate([out_grad, terms], axis=1)
+
+
 def local(query_rows, key_rows, value_rows, out_grad, log_totals, out_dot, bias_table):
     rows, feats = query_rows.shape
     heads = log_totals.shape[1]
     table_len = bias_table.shape[1]
     half = rows // 2
     pair_flops = 2 * rows * rows * feats
+    vmem = pl.BlockSpec(memory_space=pltpu.VMEM)
+    hbm = pl.BlockSpec(memory_space=pltpu.HBM)
 
     def cost(matmuls):
         return pl.CostEstimate(
@@ -273,21 +313,22 @@
             transcendentals=heads * rows * rows,
         )
 
-    def call(body, matmuls, outs, *args):
+    def call(body, matmuls, outs, args, scratch=(), specs=None):
         return pl.pallas_call(
             body,
-            in_specs=[pl.BlockSpec(memory_space=pltpu.VMEM)] * len(args),
-            out_specs=[pl.BlockSpec(memory_space=pltpu.VMEM)] * len(outs),
+            in_specs=[vmem] * len(args) if specs is None else specs,
+            out_specs=[vmem] * len(outs),
             out_shape=outs,
+            scratch_shapes=list(scratch),
             cost_estimate=cost(matmuls),
             compiler_params=pltpu.CompilerParams(vmem_limit_bytes=16 * 2**20),
         )(*args)
 
+    grads = packed_grads(out_grad, log_totals, out_dot)
     moved = {}
-    stats = jnp.concatenate([log_totals * LOG2E, out_dot], axis=1).T
     for lag in (1, 2):
         parts = []
-        for part in (query_rows, out_grad, stats):
+        for part in (query_rows, grads):
             parts.append(shifted(part, -lag))
         moved[lag] = parts
 
@@ -295,43 +336,46 @@
     rows_b16 = pltpu.VMEM((rows, feats), BF16)
     turn_f32 = pltpu.VMEM((feats, rows), F32)
     turn_b16 = pltpu.VMEM((feats, rows), BF16)
-    tab_shape = pltpu.VMEM((heads, 4 * half), F32)
+    wide_tab = pltpu.VMEM((heads, 4 * half), F32)
+    table_shape = pltpu.VMEM((heads, table_len), F32)
     sq_shape = pltpu.VMEM((heads, rows, rows), BF16)
     tile_shape = pltpu.VMEM((heads, 3, half, half), F32)
+    stat_shape = pltpu.VMEM((2 * heads, rows), F32)
+    out_shape = jax.ShapeDtypeStruct((rows, feats), BF16)
 
     body = functools.partial
-    dq0, dk, dv, tab, turned, tiles, chunks = call(
+    dq0, dk, dv, tab, turned, tiles, chunks, keys, values = call(
         body(lag_kernel, 0, 2, heads), 5,
-        [turn_f32, rows_f32, rows_f32, tab_shape, turn_b16, tile_shape, tab_shape],
-        key_rows, value_rows, query_rows, out_grad, stats, bias_table,
+        [turn_f32, rows_f32, rows_f32, wide_tab, turn_b16, tile_shape, wide_tab,
+         rows_b16, rows_b16],
+        (key_rows, value_rows, query_rows, grads, bias_table),
+        (rows_b16, table_shape, stat_shape, pltpu.SemaphoreType.DMA((4,))),
+        [hbm, hbm, hbm, vmem, hbm],
     )
     dq2, dk, dv, tab = call(
         body(lag_kernel, 2, 2, heads), 5,
-        [turn_b16, rows_f32, rows_f32, tab_shape],
-        key_rows, value_rows, *moved[2], turned, tiles, chunks, dk, dv, tab,
+        [turn_b16, rows_f32, rows_f32, wide_tab],
+        (keys, values, *moved[2], turned, tiles, chunks, dk, dv, tab),
+        (stat_shape,),
     )
     back2 = shifted(dq2, 2)
-    dq1, tab, weights, scores = call(
+    dq1, table_part, weights, scores = call(
         body(lag_kernel, 1, 2, heads), 3,
-        [turn_b16, tab_shape, sq_shape, sq_shape],
-        key_rows, value_rows, *moved[1], turned, tiles, chunks, tab,
+        [turn_b16, table_shape, sq_shape, sq_shape],
+        (keys, values, *moved[1], turned, tiles, chunks, tab),
+        (wide_tab, stat_shape),
     )
     back1 = shifted(dq1, 1)
-    lines = all_sum(tab)
-    out_shape = jax.ShapeDtypeStruct((rows, feats), BF16)
-    grad_key, grad_value = call(
-        body(close_kernel, 2), 2, [out_shape, out_shape],
-        weights, scores, moved[1][0], moved[1][1], dk, dv,
-    )
-    grad_query, = call(body(query_kernel, 2, heads), 1, [out_shape], dq0, back1, back2)
-    start = half - (SEG_LEN - 1)
-    grad_table = jnp.concatenate(
-        [
-            lines[:, start : start + table_len - 1],
-            jnp.sum(lines[:, start + table_len - 1 :], axis=1, keepdims=True),
-        ],
-        axis=1,
-    )
+    grad_table = all_sum(table_part)
+    grad_key, = call(
+        body(close_kernel, 2, True), 1, [out_shape],
+        (scores, moved[1][0], dk),
+    )
+    grad_value, = call(
+        body(close_kernel, 2, False), 1, [out_shape],
+        (weights, moved[1][1], dv),
+    )
+    grad_query, = call(body(query_kernel, 2, heads), 1, [out_shape], (dq0, back1, back2))
     return grad_query, grad_key, grad_value, grad_table
 
 

time: 73.4 us -> 71.9 us (0.980)
  starting transfers between devices: 38.9 us -> 21.3 us
  waiting for transfers between devices: 11.4 us -> 28.9 us
  local copies, waits for them, and re-layouts: 5.02 us -> 1.17 us
  Pallas kernels: 14.4 us -> 16.1 us
  other arithmetic: 2.21 us -> 3.2 us
    ppermute x10 -> x7, starting transfers between devices: 25.3 us -> 9.29 us  [all_sum(): parts.append(lax.ppermute(part, AXES, route))]
    ppermute x10 -> x7, waiting for transfers between devices: 2.15 us -> 12 us  [all_sum(): parts.append(lax.ppermute(part, AXES, route))]
    ppermute x8 -> x6, waiting for transfers between devices: 9.28 us -> 17 us  [shifted(): return lax.ppermute(block, AXES, route)]
    unnamed x10 -> x8, local copies, waits for them, and re-layouts: 4.87 us -> 1.05 us
    pallas_call x5 -> x6, Pallas kernels: 14.4 us -> 16.1 us  [call(): pl.pallas_call(body, in_specs=[vmem] * len(args) if specs is None else sp...]
    ppermute x8 -> x6, starting transfers between devices: 13.6 us -> 12 us  [shifted(): return lax.ppermute(block, AXES, route)]
  transfers between devices with their start and end apart: 18 -> 13, of which waited for: 3 -> 6; matrix products, arithmetic and copies ran while one was open for 3% -> 1% of each run, Pallas kernels for 14% -> 16%
where the time goes in v3:
time: 71.9 us; the launch traced here: 71.5 us
  waiting for transfers between devices  28.9 us (40%)
  starting transfers between devices  21.3 us (30%)
  Pallas kernels  16.1 us (22%)
  other arithmetic  3.2 us (4%)
  local copies, waits for them, and re-layouts  1.17 us (2%)
  between operations  0.79 us (1%)
    ppermute x6, waiting for transfers between devices, shifted(): return lax.ppermute(block, AXES, route)  17 us
    pallas_call x6, Pallas kernels, call(): pl.pallas_call(body, in_specs=[vmem] * len(args) if specs is None else sp...  16.1 us
    ppermute x6, starting transfers between devices, shifted(): return lax.ppermute(block, AXES, route)  12 us
    ppermute x7, waiting for transfers between devices, all_sum(): parts.append(lax.ppermute(part, AXES, route))  12 us
    ppermute x7, starting transfers between devices, all_sum(): parts.append(lax.ppermute(part, AXES, route))  9.29 us
  transfers between devices with their start and end apart: 13, of which 6 were waited for; matrix products, arithmetic and copies ran while one was open for 1% of the time, Pallas kernels for 16%

profile of v3, /device:TPU:0, one launch (start us, length us, event | category | flops | bytes accessed | tf_op | source)
XLA Modules:
  0.0 71.5 jit_solution(8909227051377591887)
XLA Ops:
  0.7 0.8 %broadcast_multiply_fusion = f32[256,8]{0,1:T(8,128)S(1)} fusion(f32[256,8]{0,1:T(8,128)} %param.11), kind=kLoop, calls=%fused_computation.12 | loop fusion | flops 2048 | bytes 16384 | tf_op jit(solution)/shard_map/mul | solution.py:291
  1.4 0.7 reduce-precision_convert_fusion.1
  2.2 0.1 copy.14
  2.3 1.1 %fusion.1.refs_3_ = bf16[256,1152]{1,0:T(8,128)(2,1)S(1)} fusion(bf16[256,48]{1,0:T(8,128)(2,1)S(1)} %copy.14, bf16[256,1024]{1,0:T(8,128)(2,1)} %param.10), kind=kLoop, calls=%fused_computation.2 | loop fusion | flops 1769472 | bytes 1138688 | tf_op jit(solution)/shard_map/concatenate | solution.py:297
  3.4 1.3 %collective-permute-start.3 = (bf16[256,1152]{1,0:T(8,128)(2,1)S(1)}, bf16[256,1152]{1,0:T(8,128)(2,1)S(1)}, u32[]{:S(2)}, u32[]{:S(2)}) collective-permute-start(bf16[256,1152]{1,0:T(8,128)(2,1)S(1)} %fusion.1.refs_3_), channel_id=1, source_target_pairs={{2,0},{3,1},{4,2},{5,3},{6,4},{7,5},{8,6},{9,7},{10,8},{11,9},{12,... | collective-permute-start | bytes 1769480 | tf_op jit(solution)/shard_map/ppermute | solution.py:26
  4.7 1.3 %collective-permute-start.1 = (bf16[256,1152]{1,0:T(8,128)(2,1)S(1)}, bf16[256,1152]{1,0:T(8,128)(2,1)S(1)}, u32[]{:S(2)}, u32[]{:S(2)}) collective-permute-start(bf16[256,1152]{1,0:T(8,128)(2,1)S(1)} %fusion.1.refs_3_), channel_id=1, source_target_pairs={{1,0},{2,1},{3,2},{4,3},{5,4},{6,5},{7,6},{8,7},{9,8},{10,9},{11,1... | collective-permute-start | bytes 1769480 | tf_op jit(solution)/shard_map/ppermute | solution.py:26
  6.0 1.3 %collective-permute-start.2 = (bf16[256,1024]{1,0:T(8,128)(2,1)}, bf16[256,1024]{1,0:T(8,128)(2,1)S(1)}, u32[]{:S(2)}, u32[]{:S(2)}) collective-permute-start(bf16[256,1024]{1,0:T(8,128)(2,1)} %refs_2_.1), channel_id=1, source_target_pairs={{2,0},{3,1},{4,2},{5,3},{6,4},{7,5},{8,6},{9,7},{10,8},{11,9},{12,... | collective-permute-start | bytes 1572872 | tf_op jit(solution)/shard_map/ppermute | solution.py:26
  7.3 1.3 %collective-permute-start = (bf16[256,1024]{1,0:T(8,128)(2,1)}, bf16[256,1024]{1,0:T(8,128)(2,1)S(1)}, u32[]{:S(2)}, u32[]{:S(2)}) collective-permute-start(bf16[256,1024]{1,0:T(8,128)(2,1)} %refs_2_.1), channel_id=1, source_target_pairs={{1,0},{2,1},{3,2},{4,3},{5,4},{6,5},{7,6},{8,7},{9,8},{10,9},{11,1... | collective-permute-start | bytes 1572872 | tf_op jit(solution)/shard_map/ppermute | solution.py:26
  8.6 0.0 copy-start.2
  8.6 1.0 %copy-done.2 = bf16[256,1024]{1,0:T(8,128)(2,1)S(1)} copy-done((bf16[256,1024]{1,0:T(8,128)(2,1)S(1)}, bf16[256,1024]{1,0:T(8,128)(2,1)}, u32[]{:S(2)}) %copy-start.2) | copy-done | bytes 524312
  9.6 4.8 %shard_map.102 = (f32[1024,256]{1,0:T(8,128)S(1)}, f32[256,1024]{1,0:T(8,128)S(1)}, f32[256,1024]{1,0:T(8,128)S(1)}, f32[8,512]{1,0:T(8,128)S(1)}, bf16[1024,256...) custom-call(bf16[256,1024]{1,0:T(8,128)(2,1)S(1)} %copy-done, ...), custom_call_target="tpu_custom_call" | custom-call | flops 671088640 | bytes 2097152 | tf_op jit(solution)/shard_map/pallas_call | solution.py:317
  14.4 3.1 %shard_map.103 = (bf16[1024,256]{1,0:T(8,128)(2,1)S(1)}, f32[256,1024]{1,0:T(8,128)S(1)}, f32[256,1024]{1,0:T(8,128)S(1)}, f32[8,512]{1,0:T(8,128)S(1)}) custom-call(bf16[256,1024]{1,0:T(8,128)(2,1)S(1)} %get-tuple-element.22.refs_0_, bf16[256,1024]{1,0:T(8,128)(2,1)S(1)} %get-tuple-element.23.refs_1_, bf16[256,1024]{1,0:T(8,128)(2,1)S(1)} %collective-permute-done.2.refs_2_, ...), custom_call_target="tpu_custom_call" | custom-call | flops 671088640 | bytes 2097152 | tf_op jit(solution)/shard_map/pallas_call | solution.py:317
  17.6 16.9 %collective-permute-done.refs_2_.x_ref = bf16[256,1024]{1,0:T(8,128)(2,1)S(1)} collective-permute-done((bf16[256,1024]{1,0:T(8,128)(2,1)}, bf16[256,1024]{1,0:T(8,128)(2,1)S(1)}, u32[]{:S(2)}, u32[]{:S(2)}) %collective-permute-start) | collective-permute-done | bytes 524320 | tf_op jit(solution)/shard_map/ppermute | solution.py:26
  34.5 3.3 %shard_map.104 = (bf16[1024,256]{1,0:T(8,128)(2,1)S(1)}, f32[8,320]{1,0:T(8,128)S(1)}, bf16[8,256,256]{2,1,0:T(8,128)(2,1)S(1)}, bf16[8,256,256]{2,1,0:T(8,128)(2,1)S(1)}) custom-call(bf16[256,1024]{1,0:T(8,128)(2,1)S(1)} %get-tuple-element.22.refs_0_, bf16[256,1024]{1,0:T(8,128)(2,1)S(1)} %get-tuple-element.23.refs_1_, ...), custom_call_target="tpu_custom_call" | custom-call | flops 402653184 | bytes 2097152 | tf_op jit(solution)/shard_map/pallas_call | solution.py:317
  37.9 1.6 %collective-permute-start.4 = (bf16[1024,256]{1,0:T(8,128)(2,1)S(1)}, bf16[1024,256]{1,0:T(8,128)(2,1)S(1)}, u32[]{:S(2)}, u32[]{:S(2)}) collective-permute-start(bf16[1024,256]{1,0:T(8,128)(2,1)S(1)} %get-tuple-element.31), channel_id=1, source_target_pairs={{0,1},{1,2},{2,3},{3,4},{4,5},{5,6},{6,7},{7,8},{8,9},{9,10},{10,1... | collective-permute-start | bytes 1572872 | tf_op jit(solution)/shard_map/ppermute | solution.py:26
  39.5 5.3 %collective-permute-start.5 = (bf16[1024,256]{1,0:T(8,128)(2,1)S(1)}, bf16[1024,256]{1,0:T(8,128)(2,1)S(1)}, u32[]{:S(2)}, u32[]{:S(2)}) collective-permute-start(bf16[1024,256]{1,0:T(8,128)(2,1)S(1)} %get-tuple-element.32), channel_id=1, source_target_pairs={{0,2},{1,3},{2,4},{3,5},{4,6},{5,7},{6,8},{7,9},{8,10},{9,11},{10,... | collective-permute-start | bytes 1572872 | tf_op jit(solution)/shard_map/ppermute | solution.py:26
  44.8 1.3 %collective-permute-start.6 = (f32[8,320]{1,0:T(8,128)S(1)}, f32[8,320]{1,0:T(8,128)S(1)}, u32[]{:S(2)}, u32[]{:S(2)}) collective-permute-start(f32[8,320]{1,0:T(8,128)S(1)} %get-tuple-element.37), channel_id=1, source_target_pairs={{0,1},{1,0},{2,3},{3,2},{4,5},{5,4},{6,7},{7,6},{8,9},{9,8},{10,11... | collective-permute-start | bytes 30728 | tf_op jit(solution)/shard_map/ppermute | solution.py:63
  46.0 7.0 %collective-permute-done.6 = f32[8,320]{1,0:T(8,128)S(1)} collective-permute-done((f32[8,320]{1,0:T(8,128)S(1)}, f32[8,320]{1,0:T(8,128)S(1)}, u32[]{:S(2)}, u32[]{:S(2)}) %collective-permute-start.6) | collective-permute-done | bytes 10272 | tf_op jit(solution)/shard_map/ppermute | solution.py:63
  53.1 1.5 %collective-permute-start.7 = (f32[8,320]{1,0:T(8,128)S(1)}, f32[8,320]{1,0:T(8,128)S(1)}, u32[]{:S(2)}, u32[]{:S(2)}) collective-permute-start(f32[8,320]{1,0:T(8,128)S(1)} %add.23), channel_id=1, source_target_pairs={{0,2},{1,3},{2,0},{3,1},{4,6},{5,7},{6,4},{7,5},{8,10},{9,11},{10,... | collective-permute-start | bytes 30728 | tf_op jit(solution)/shard_map/ppermute | solution.py:63
  54.6 1.3 %collective-permute-start.8 = (f32[8,320]{1,0:T(8,128)S(1)}, f32[8,320]{1,0:T(8,128)S(1)}, u32[]{:S(2)}, u32[]{:S(2)}) collective-permute-start(f32[8,320]{1,0:T(8,128)S(1)} %add.23), channel_id=1, source_target_pairs={{0,4},{1,5},{2,6},{3,7},{4,0},{5,1},{6,2},{7,3},{8,12},{9,13},{10,... | collective-permute-start | bytes 30728 | tf_op jit(solution)/shard_map/ppermute | solution.py:63
  55.9 0.1 collective-permute-start.9
  55.9 1.7 %shard_map.107 = bf16[256,1024]{1,0:T(8,128)(2,1)} custom-call(bf16[8,256,256]{2,1,0:T(8,128)(2,1)S(1)} %get-tuple-element.35.w_ref, bf16[256,1152]{1,0:T(8,128)(2,1)S(1)} %collective-permute-done.1.refs_3_.x_ref, f32[256,1024]{1,0:T(8,128)S(1)} %get-tuple-element.36.part_ref), custom_call_target="tpu_custom_call" | custom-call | flops 134217728 | bytes 2097152 | tf_op jit(solution)/shard_map/pallas_call | solution.py:317
  57.7 0.6 collective-permute-done.8
  58.3 0.8 %collective-permute-done.9 = f32[8,320]{1,0:T(8,128)S(1)} collective-permute-done((f32[8,320]{1,0:T(8,128)S(1)}, f32[8,320]{1,0:T(8,128)S(1)}, u32[]{:S(2)}, u32[]{:S(2)}) %collective-permute-start.9) | collective-permute-done | bytes 10272 | tf_op jit(solution)/shard_map/ppermute | solution.py:63
  59.0 2.7 %collective-permute-start.10 = (f32[8,320]{1,0:T(8,128)S(1)}, f32[8,320]{1,0:T(8,128)S(1)}, u32[]{:S(2)}, u32[]{:S(2)}) collective-permute-start(f32[8,320]{1,0:T(8,128)S(1)} %add_add_fusion.1), channel_id=1, source_target_pairs={{0,8},{1,9},{2,10},{3,11},{4,12},{5,13},{6,14},{7,15},{8,0},{9,1},... | collective-permute-start | bytes 30728 | tf_op jit(solution)/shard_map/ppermute | solution.py:63
  61.7 2.4 %collective-permute-start.11 = (f32[8,320]{1,0:T(8,128)S(1)}, f32[8,320]{1,0:T(8,128)S(1)}, u32[]{:S(2)}, u32[]{:S(2)}) collective-permute-start(f32[8,320]{1,0:T(8,128)S(1)} %add_add_fusion.1), channel_id=1, source_target_pairs={{0,16},{1,17},{2,18},{3,19},{4,20},{5,21},{6,22},{7,23},{8,24},{9,... | collective-permute-start | bytes 30728 | tf_op jit(solution)/shard_map/ppermute | solution.py:63
  64.1 0.1 collective-permute-start.12
  64.2 1.8 %shard_map.106 = bf16[256,1024]{1,0:T(8,128)(2,1)} custom-call(bf16[8,256,256]{2,1,0:T(8,128)(2,1)S(1)} %get-tuple-element.33.w_ref, bf16[256,1024]{1,0:T(8,128)(2,1)S(1)} %collective-permute-done.refs_2_.x_ref, f32[256,1024]{1,0:T(8,128)S(1)} %get-tuple-element.34.part_ref), custom_call_target="tpu_custom_call" | custom-call | flops 134217728 | bytes 2097152 | tf_op jit(solution)/shard_map/pallas_call | solution.py:317
  66.0 0.3 collective-permute-done.11
  66.3 3.3 %collective-permute-done.12 = f32[8,320]{1,0:T(8,128)S(1)} collective-permute-done((f32[8,320]{1,0:T(8,128)S(1)}, f32[8,320]{1,0:T(8,128)S(1)}, u32[]{:S(2)}, u32[]{:S(2)}) %collective-permute-start.12) | collective-permute-done | bytes 10272 | tf_op jit(solution)/shard_map/ppermute | solution.py:63
  69.6 0.6 add_add_fusion
  70.2 1.3 %shard_map.105 = bf16[256,1024]{1,0:T(8,128)(2,1)} custom-call(f32[1024,256]{1,0:T(8,128)S(1)} %get-tuple-element.21.dq_ref, bf16[1024,256]{1,0:T(8,128)(2,1)S(1)} %collective-permute-done.4.one_ref, bf16[1024,256]{1,0:T(8,128)(2,1)S(1)} %collective-permute-done.5.two_ref), custom_call_target="tpu_custom_call" | custom-call | flops 134217728 | bytes 2097152 | tf_op jit(solution)/shard_map/pallas_call | solution.py:317
  (16 shorter events, 0.0 us)
Async XLA Ops:
  0.6 7.9 %copy-start.3 = (f32[8,320]{1,0:T(8,128)S(1)}, f32[8,320]{1,0:T(8,128)}, u32[]{:S(2)}) copy-start(f32[8,320]{1,0:T(8,128)} %refs_4_.1) | copy-start | bytes 30724
  0.6 7.9 %copy-start = (bf16[256,1024]{1,0:T(8,128)(2,1)S(1)}, bf16[256,1024]{1,0:T(8,128)(2,1)}, u32[]{:S(2)}) copy-start(bf16[256,1024]{1,0:T(8,128)(2,1)} %refs_0_.1) | copy-start | bytes 1572868
  0.7 7.9 %copy-start.1 = (bf16[256,1024]{1,0:T(8,128)(2,1)S(1)}, bf16[256,1024]{1,0:T(8,128)(2,1)}, u32[]{:S(2)}) copy-start(bf16[256,1024]{1,0:T(8,128)(2,1)} %refs_1_.1) | copy-start | bytes 1572868
  3.4 11.1 %collective-permute-start.3 = (bf16[256,1152]{1,0:T(8,128)(2,1)S(1)}, bf16[256,1152]{1,0:T(8,128)(2,1)S(1)}, u32[]{:S(2)}, u32[]{:S(2)}) collective-permute-start(bf16[256,1152]{1,0:T(8,128)(2,1)S(1)} %fusion.1.refs_3_), channel_id=1, source_target_pairs={{2,0},{3,1},{4,2},{5,3},{6,4},{7,5},{8,6},{9,7},{10,8},{11,9},{12,... | collective-permute-start | bytes 1769480 | tf_op jit(solution)/shard_map/ppermute | solution.py:26
  4.7 29.8 %collective-permute-start.1 = (bf16[256,1152]{1,0:T(8,128)(2,1)S(1)}, bf16[256,1152]{1,0:T(8,128)(2,1)S(1)}, u32[]{:S(2)}, u32[]{:S(2)}) collective-permute-start(bf16[256,1152]{1,0:T(8,128)(2,1)S(1)} %fusion.1.refs_3_), channel_id=1, source_target_pairs={{1,0},{2,1},{3,2},{4,3},{5,4},{6,5},{7,6},{8,7},{9,8},{10,9},{11,1... | collective-permute-start | bytes 1769480 | tf_op jit(solution)/shard_map/ppermute | solution.py:26
  6.0 8.4 %collective-permute-start.2 = (bf16[256,1024]{1,0:T(8,128)(2,1)}, bf16[256,1024]{1,0:T(8,128)(2,1)S(1)}, u32[]{:S(2)}, u32[]{:S(2)}) collective-permute-start(bf16[256,1024]{1,0:T(8,128)(2,1)} %refs_2_.1), channel_id=1, source_target_pairs={{2,0},{3,1},{4,2},{5,3},{6,4},{7,5},{8,6},{9,7},{10,8},{11,9},{12,... | collective-permute-start | bytes 1572872 | tf_op jit(solution)/shard_map/ppermute | solution.py:26
  7.3 27.2 %collective-permute-start = (bf16[256,1024]{1,0:T(8,128)(2,1)}, bf16[256,1024]{1,0:T(8,128)(2,1)S(1)}, u32[]{:S(2)}, u32[]{:S(2)}) collective-permute-start(bf16[256,1024]{1,0:T(8,128)(2,1)} %refs_2_.1), channel_id=1, source_target_pairs={{1,0},{2,1},{3,2},{4,3},{5,4},{6,5},{7,6},{8,7},{9,8},{10,9},{11,1... | collective-permute-start | bytes 1572872 | tf_op jit(solution)/shard_map/ppermute | solution.py:26
  8.6 1.0 %copy-start.2 = (bf16[256,1024]{1,0:T(8,128)(2,1)S(1)}, bf16[256,1024]{1,0:T(8,128)(2,1)}, u32[]{:S(2)}) copy-start(bf16[256,1024]{1,0:T(8,128)(2,1)} %refs_2_.1) | copy-start | bytes 1572868
  37.9 32.3 %collective-permute-start.4 = (bf16[1024,256]{1,0:T(8,128)(2,1)S(1)}, bf16[1024,256]{1,0:T(8,128)(2,1)S(1)}, u32[]{:S(2)}, u32[]{:S(2)}) collective-permute-start(bf16[1024,256]{1,0:T(8,128)(2,1)S(1)} %get-tuple-element.31), channel_id=1, source_target_pairs={{0,1},{1,2},{2,3},{3,4},{4,5},{5,6},{6,7},{7,8},{8,9},{9,10},{10,1... | collective-permute-start | bytes 1572872 | tf_op jit(solution)/shard_map/ppermute | solution.py:26
  39.5 30.7 %collective-permute-start.5 = (bf16[1024,256]{1,0:T(8,128)(2,1)S(1)}, bf16[1024,256]{1,0:T(8,128)(2,1)S(1)}, u32[]{:S(2)}, u32[]{:S(2)}) collective-permute-start(bf16[1024,256]{1,0:T(8,128)(2,1)S(1)} %get-tuple-element.32), channel_id=1, source_target_pairs={{0,2},{1,3},{2,4},{3,5},{4,6},{5,7},{6,8},{7,9},{8,10},{9,11},{10,... | collective-permute-start | bytes 1572872 | tf_op jit(solution)/shard_map/ppermute | solution.py:26
  44.8 8.3 %collective-permute-start.6 = (f32[8,320]{1,0:T(8,128)S(1)}, f32[8,320]{1,0:T(8,128)S(1)}, u32[]{:S(2)}, u32[]{:S(2)}) collective-permute-start(f32[8,320]{1,0:T(8,128)S(1)} %get-tuple-element.37), channel_id=1, source_target_pairs={{0,1},{1,0},{2,3},{3,2},{4,5},{5,4},{6,7},{7,6},{8,9},{9,8},{10,11... | collective-permute-start | bytes 30728 | tf_op jit(solution)/shard_map/ppermute | solution.py:63
  53.1 4.6 %collective-permute-start.7 = (f32[8,320]{1,0:T(8,128)S(1)}, f32[8,320]{1,0:T(8,128)S(1)}, u32[]{:S(2)}, u32[]{:S(2)}) collective-permute-start(f32[8,320]{1,0:T(8,128)S(1)} %add.23), channel_id=1, source_target_pairs={{0,2},{1,3},{2,0},{3,1},{4,6},{5,7},{6,4},{7,5},{8,10},{9,11},{10,... | collective-permute-start | bytes 30728 | tf_op jit(solution)/shard_map/ppermute | solution.py:63
  54.6 3.7 %collective-permute-start.8 = (f32[8,320]{1,0:T(8,128)S(1)}, f32[8,320]{1,0:T(8,128)S(1)}, u32[]{:S(2)}, u32[]{:S(2)}) collective-permute-start(f32[8,320]{1,0:T(8,128)S(1)} %add.23), channel_id=1, source_target_pairs={{0,4},{1,5},{2,6},{3,7},{4,0},{5,1},{6,2},{7,3},{8,12},{9,13},{10,... | collective-permute-start | bytes 30728 | tf_op jit(solution)/shard_map/ppermute | solution.py:63
  55.9 3.2 %collective-permute-start.9 = (f32[8,320]{1,0:T(8,128)S(1)}, f32[8,320]{1,0:T(8,128)S(1)}, u32[]{:S(2)}, u32[]{:S(2)}) collective-permute-start(f32[8,320]{1,0:T(8,128)S(1)} %add.23), channel_id=1, source_target_pairs={{0,6},{1,7},{2,4},{3,5},{4,2},{5,3},{6,0},{7,1},{8,14},{9,15},{10,... | collective-permute-start | bytes 30728 | tf_op jit(solution)/shard_map/ppermute | solution.py:63
  59.0 7.0 %collective-permute-start.10 = (f32[8,320]{1,0:T(8,128)S(1)}, f32[8,320]{1,0:T(8,128)S(1)}, u32[]{:S(2)}, u32[]{:S(2)}) collective-permute-start(f32[8,320]{1,0:T(8,128)S(1)} %add_add_fusion.1), channel_id=1, source_target_pairs={{0,8},{1,9},{2,10},{3,11},{4,12},{5,13},{6,14},{7,15},{8,0},{9,1},... | collective-permute-start | bytes 30728 | tf_op jit(solution)/shard_map/ppermute | solution.py:63
  61.7 4.6 %collective-permute-start.11 = (f32[8,320]{1,0:T(8,128)S(1)}, f32[8,320]{1,0:T(8,128)S(1)}, u32[]{:S(2)}, u32[]{:S(2)}) collective-permute-start(f32[8,320]{1,0:T(8,128)S(1)} %add_add_fusion.1), channel_id=1, source_target_pairs={{0,16},{1,17},{2,18},{3,19},{4,20},{5,21},{6,22},{7,23},{8,24},{9,... | collective-permute-start | bytes 30728 | tf_op jit(solution)/shard_map/ppermute | solution.py:63
  64.1 5.5 %collective-permute-start.12 = (f32[8,320]{1,0:T(8,128)S(1)}, f32[8,320]{1,0:T(8,128)S(1)}, u32[]{:S(2)}, u32[]{:S(2)}) collective-permute-start(f32[8,320]{1,0:T(8,128)S(1)} %add_add_fusion.1), channel_id=1, source_target_pairs={{0,24},{1,25},{2,26},{3,27},{4,28},{5,29},{6,30},{7,31},{8,16},{9,... | collective-permute-start | bytes 30728 | tf_op jit(solution)/shard_map/ppermute | solution.py:63

commit v4 on v3

v4 whole, which is shorter than its diff:
```python
import functools
import math

import jax
import jax.numpy as jnp
from jax import lax
from jax.experimental import pallas as pl
from jax.experimental.pallas import tpu as pltpu
from jax.sharding import PartitionSpec as P


SEG_LEN = 64
AXES = ("sp", "tp")
LOG2E = math.log2(math.e)
MASKED = -1e30
TERMS = 3
ROUND_ORDER = ((1,), (3, 4), (0, 2))
F32 = jnp.float32
BF16 = jnp.bfloat16
NT = (((1,), (1,)), ((), ()))
NN = (((1,), (0,)), ((), ()))


def shifted(block, distance):
    count = lax.axis_size(AXES)
    route = [(i - distance, i) for i in range(count) if 0 <= i - distance < count]
    return lax.ppermute(block, AXES, route)


def pair_tree(parts):
    while len(parts) > 1:
        parts = [parts[i] + parts[i + 1] for i in range(0, len(parts), 2)]
    return parts[0]


def table_rounds(count):
    twos = []
    stride = 1
    while count % (2 * stride) == 0:
        twos.append(stride)
        stride *= 2
    order = ROUND_ORDER
    rounds = [tuple(twos[d] for d in digits if d < len(twos)) for digits in order]
    used = sum(len(digits) for digits in order)
    rounds += [(twos[d],) for d in range(used, len(twos))]
    odd = []
    rest, factor = count // stride, 3
    while rest > 1:
        while rest % factor == 0:
            odd.append((stride, factor))
            stride *= factor
            rest //= factor
        factor += 2
    return [r for r in rounds if r], odd


def all_sum(part):
    count = lax.axis_size(AXES)
    me = lax.axis_index(AXES)
    binary, odd = table_rounds(count)
    for strides in binary:
        masks = [0]
        for stride in strides:
            masks += [mask ^ stride for mask in masks]
        parts = [part]
        for mask in masks[1:]:
            parts.append(lax.ppermute(part, AXES, [(i, i ^ mask) for i in range(count)]))
        part = pair_tree(parts)
    for stride, radix in odd:
        digit = (me // stride) % radix
        parts = [part]
        for step in range(1, radix):
            route = []
            for i in range(count):
                d = (i // stride) % radix
                route.append((i, i + (((d - step) % radix) - d) * stride))
            parts.append(lax.ppermute(part, AXES, route))
        total = jnp.zeros_like(part)
        for d in range(radix):
            value = parts[0]
            for step in range(1, radix):
                value = jnp.where((digit + step) % radix == d, parts[step], value)
            total = total + value
        part = total
    return part


def prep_tiles(head_count, table_ref, chunk_ref, tile_ref):
    size = tile_ref.shape[2]
    table_len = table_ref.shape[1]
    span = chunk_ref.shape[1]
    pad = size - (SEG_LEN - 1)
    lane = lax.broadcasted_iota(jnp.int32, (head_count, span), 1)
    table = table_ref[...] * LOG2E
    first, last = table[:, :1], table[:, table_len - 1 :]
    wide = jnp.concatenate([table, jnp.zeros((head_count, span - table_len), F32)], axis=1)
    moved = pltpu.roll(wide, pad, 1)
    moved = jnp.where(lane < pad, first, jnp.where(lane >= pad + table_len, last, moved))
    chunk_ref[...] = moved
    row = lax.broadcasted_iota(jnp.int32, (size, size), 0)
    col = lax.broadcasted_iota(jnp.int32, (size, size), 1)

    @pl.loop(0, head_count)
    def _(head):
        rolled = []
        lines = chunk_ref[pl.ds(head, 1), :]
        for c in range(4):
            line = jnp.broadcast_to(lines[:, c * size : (c + 1) * size], (size, size))
            rolled.append(pltpu.roll(line, 0, 1, stride=1, stride_axis=0))
        for b in range(3):
            tile = jnp.where(col >= row, rolled[b + 1], rolled[b])
            if b == 0:
                tile = jnp.where((row // SEG_LEN) <= (col // SEG_LEN), tile, MASKED)
            tile_ref[head, b] = tile


def unroll_sum(tile):
    size = tile.shape[0]
    group = 8
    parts = []
    for start in range(0, size, group):
        part = tile[start : start + group, :]
        parts.append(part if start == 0 else pltpu.roll(part, size - start, 1))
    total = pair_tree(parts)
    row = lax.broadcasted_iota(jnp.int32, total.shape, 0)
    for bit in (1, 2, 4):
        total = jnp.where((row & bit) != 0, pltpu.roll(total, size - bit, 1), total)
    return jnp.sum(total, axis=0, keepdims=True)


def score_terms(lag, key, value, query, grad, log_row, dot_row, tiles, const, inv_root):
    rows = key.shape[0]
    half = rows // 2
    raw = lax.dot_general(key, query, NT, preferred_element_type=F32)
    wgt = lax.dot_general(value, grad, NT, preferred_element_type=F32)
    row = lax.broadcasted_iota(jnp.int32, (half, half), 0) // SEG_LEN
    col = lax.broadcasted_iota(jnp.int32, (half, half), 1) // SEG_LEN
    acc = [None, None, None, None]
    w_rows, s_rows = [], []
    for r in range(2):
        w_cols, s_cols = [], []
        for c in range(2):
            if (lag == 0 and r > c) or (lag == 2 and c > r):
                w_cols.append(jnp.zeros((half, half), BF16))
                s_cols.append(jnp.zeros((half, half), BF16))
                continue
            rs, cs = slice(r * half, (r + 1) * half), slice(c * half, (c + 1) * half)
            level = min(2 * lag + c - r, 3)
            lrow = log_row[:, cs]
            bias = const - lrow if level == 3 else tiles[level] - lrow
            weight = jnp.exp2(raw[rs, cs] * (inv_root * LOG2E) + bias)
            if lag == 2 and r == c:
                weight = jnp.where(col <= row, weight, 0.0)
            score = weight * (wgt[rs, cs] - dot_row[:, cs])
            acc[level] = score if acc[level] is None else acc[level] + score
            w_cols.append(weight.astype(BF16))
            s_cols.append(score.astype(BF16))
        w_rows.append(jnp.concatenate(w_cols, axis=1))
        s_rows.append(jnp.concatenate(s_cols, axis=1))
    return jnp.concatenate(w_rows, axis=0), jnp.concatenate(s_rows, axis=0), acc


def table_lines(acc, size):
    row = lax.broadcasted_iota(jnp.int32, (size, size), 0)
    col = lax.broadcasted_iota(jnp.int32, (size, size), 1)
    zero = jnp.zeros((size, size), F32)
    lines = []
    for c in range(4):
        upper = acc[c - 1] if c > 0 else None
        lower = acc[c] if c < 3 else None
        line = None
        if upper is not None or lower is not None:
            mixed = jnp.where(
                col >= row,
                zero if upper is None else upper,
                zero if lower is None else lower,
            )
            line = unroll_sum(mixed)
        if c == 3 and acc[3] is not None:
            extra = jnp.sum(acc[3], axis=0, keepdims=True)
            line = extra if line is None else line + extra
        lines.append(line)
    return lines


def fold_table(lines, table_len, size):
    pad = size - (SEG_LEN - 1)
    lane = lax.broadcasted_iota(jnp.int32, lines.shape, 1)
    tail = jnp.sum(jnp.where(lane >= pad + table_len - 1, lines, 0.0), axis=1, keepdims=True)
    moved = pltpu.roll(lines, lines.shape[1] - pad, 1)[:, :table_len]
    lane = lax.broadcasted_iota(jnp.int32, moved.shape, 1)
    return jnp.where(lane == table_len - 1, tail, moved)


def pack_height(count, rows, width):
    lines = -(-count * TERMS * rows // width)
    return -(-lines // 8) * 8


def pack_lines(stats, width):
    count, rows = stats.shape
    high = stats.astype(BF16).astype(F32)
    rest = stats - high
    mid = rest.astype(BF16).astype(F32)
    terms = (high, mid, rest - mid)
    per_row = width // rows
    lines = []
    for line in range(pack_height(count, rows, width)):
        pieces = []
        for b in range(line * per_row, (line + 1) * per_row):
            if b < count * TERMS:
                pieces.append(terms[b // count][b % count : b % count + 1, :])
            else:
                pieces.append(jnp.zeros((1, rows), F32))
        lines.append(jnp.concatenate(pieces, axis=1))
    return jnp.concatenate(lines, axis=0).astype(BF16)


def unpack_lines(pack_ref, stat_ref):
    count, rows = stat_ref.shape
    per_row = pack_ref.shape[1] // rows
    packed = pack_ref[rows:, :].astype(F32)
    for i in range(count):
        total = None
        for term in range(TERMS):
            line, at = divmod(term * count + i, per_row)
            piece = packed[line : line + 1, at * rows : (at + 1) * rows]
            total = piece if total is None else total + piece
        stat_ref[i : i + 1, :] = total


def prep_kernel(g_hbm, log_hbm, dot_hbm, far_ref, first_ref, second_ref, stat_ref,
                log_ref, dot_ref, sems):
    rows, feats = g_hbm.shape
    cut = first_ref.shape[1]
    moves = (
        (log_hbm, log_ref),
        (dot_hbm, dot_ref),
        (g_hbm, far_ref.at[pl.ds(0, rows), :]),
        (g_hbm.at[:, pl.ds(0, cut)], first_ref.at[pl.ds(0, rows), :]),
        (g_hbm.at[:, pl.ds(cut, feats - cut)], second_ref),
    )
    copies = []
    for i, (origin, target) in enumerate(moves):
        copies.append(pltpu.make_async_copy(origin, target, sems.at[i]))
        copies[-1].start()
    for copy in copies[:2]:
        copy.wait()
    stats = jnp.concatenate([log_ref[...] * LOG2E, dot_ref[...]], axis=0)
    stat_ref[...] = stats
    first_ref[rows:, :] = pack_lines(stats, first_ref.shape[1])
    far_ref[rows:, :] = pack_lines(stats, far_ref.shape[1])
    for copy in copies[2:]:
        copy.wait()


def lag_kernel(lag, first_head, last_head, heads_step, head_count, *refs):
    if lag == 0:
        (k_hbm, v_hbm, q_hbm, table_hbm, g_ref, stat_ref,
         dq_ref, dk_ref, dv_ref, tab_ref, kt_ref, tile_ref, chunk_ref, k_ref, v_ref,
         q_ref, table_ref, sems) = refs
        pairs = ((table_hbm, table_ref), (k_hbm, k_ref), (v_hbm, v_ref), (q_hbm, q_ref))
        copies = []
        for i, (source, target) in enumerate(pairs):
            copies.append(pltpu.make_async_copy(source, target, sems.at[i]))
            copies[-1].start()
        copies[0].wait()
        prep_tiles(head_count, table_ref, chunk_ref, tile_ref)
        for copy in copies[1:]:
            copy.wait()
    elif lag == 2:
        (k_ref, v_ref, kt_ref, tile_ref, chunk_ref, dk_in, dv_in, tab_in, q_ref, g_ref,
         dk_ref, dv_ref, tab_ref, dq_ref, stat_ref) = refs
        unpack_lines(g_ref, stat_ref)
    elif first_head == 0:
        (k_ref, v_ref, kt_ref, tile_ref, chunk_ref, dk_in, dv_in, tab_in, q_ref, g_ref,
         dk_ref, dv_ref, tab_ref, dq_ref, stat_ref) = refs
        unpack_lines(g_ref, stat_ref)
    else:
        (k_ref, v_ref, kt_ref, tile_ref, chunk_ref, dk_in, dv_in, tab_in, q_ref, g_ref,
         stat_ref, _, dk_ref, dv_ref, out_tab_ref, dq_ref) = refs
    rows = k_ref.shape[0]
    size = tile_ref.shape[2]
    head_dim = k_ref.shape[1] // head_count
    inv_root = head_dim ** (-0.5)
    g_shift = -first_head * head_dim
    last_lines = []

    def one_head(local_head):
        head = local_head + first_head
        at = head * head_dim
        if not isinstance(local_head, int):
            at = pl.multiple_of(at, head_dim)
        cols = pl.ds(at, head_dim)
        key, value = k_ref[:, cols], v_ref[:, cols]
        query = q_ref[:, cols]
        grad = g_ref[:rows, pl.ds(at + g_shift, head_dim)]
        log_row = stat_ref[pl.ds(head, 1), :]
        dot_row = stat_ref[pl.ds(head + head_count, 1), :]
        const = chunk_ref[pl.ds(head, 1), :][:, 3 * size :]
        tiles = [None if lag == 2 else tile_ref[head, b] for b in range(3)]
        weights, scores, acc = score_terms(
            lag, key, value, query, grad, log_row, dot_row, tiles, const, inv_root
        )
        if lag == 0:
            turned = key.T
            kt_ref[cols, :] = turned
        else:
            turned = kt_ref[cols, :]
        dq = lax.dot_general(turned, scores, NN, preferred_element_type=F32) * inv_root
        dq_ref[cols, :] = dq.astype(dq_ref.dtype)
        lines = [
            jnp.zeros((1, size), F32) if line is None else line for line in table_lines(acc, size)
        ]
        lines = jnp.concatenate(lines, axis=1)
        if lag > 0:
            lines = tab_in[pl.ds(head, 1), :] + lines
        dk = lax.dot_general(scores, query, NN, preferred_element_type=F32)
        dv = lax.dot_general(weights, grad, NN, preferred_element_type=F32)
        if lag > 0:
            dk = dk + dk_in[:, cols]
            dv = dv + dv_in[:, cols]
        dk_ref[:, cols] = dk
        dv_ref[:, cols] = dv
        if first_head == 0:
            tab_ref[pl.ds(head, 1), :] = lines
        else:
            last_lines.append(lines)

    if first_head == 0:

        @pl.loop(0, (last_head - first_head) // heads_step)
        def _(step):
            for i in range(heads_step):
                one_head(step * heads_step + i)

    else:
        for i in range(last_head - first_head):
            one_head(i)
        table = jnp.concatenate([tab_in[:first_head, :]] + last_lines, axis=0)
        out_tab_ref[...] = fold_table(table, out_tab_ref.shape[1], size)


def close_kernel(heads_step, head_count, dq_ref, one_ref, two_ref, dk_ref, dv_ref,
                 gq_hbm, gk_hbm, gv_hbm, gq_ref, gk_ref, gv_ref, sems):
    head_dim = dq_ref.shape[0] // head_count
    inv_root = head_dim ** (-0.5)
    gk_ref[...] = (dk_ref[...] * inv_root).astype(BF16)
    copies = [pltpu.make_async_copy(gk_ref, gk_hbm, sems.at[0])]
    copies[-1].start()
    gv_ref[...] = dv_ref[...].astype(BF16)
    copies.append(pltpu.make_async_copy(gv_ref, gv_hbm, sems.at[1]))
    copies[-1].start()

    @pl.loop(0, head_count // heads_step)
    def _(step):
        for i in range(heads_step):
            cols = pl.ds(pl.multiple_of((step * heads_step + i) * head_dim, head_dim), head_dim)
            total = dq_ref[cols, :] + one_ref[cols, :].astype(F32) + two_ref[cols, :].astype(F32)
            gq_ref[:, cols] = total.T.astype(BF16)

    copies.append(pltpu.make_async_copy(gq_ref, gq_hbm, sems.at[2]))
    copies[-1].start()
    for copy in copies:
        copy.wait()


def local(query_rows, key_rows, value_rows, out_grad, log_totals, out_dot, bias_table):
    rows, feats = query_rows.shape
    heads = log_totals.shape[1]
    table_len = bias_table.shape[1]
    half = rows // 2
    cut_head = heads * 3 // 4
    head_dim = feats // heads
    cut = cut_head * head_dim
    vmem = pl.BlockSpec(memory_space=pltpu.VMEM)
    hbm = pl.BlockSpec(memory_space=pltpu.HBM)
    pair_flops = 2 * rows * rows * head_dim

    def call(body, work, outs, args, scratch=(), specs=None, out_specs=None, aliases={}):
        estimate = pl.CostEstimate(
            flops=int(work * pair_flops), bytes_accessed=8 * rows * feats, transcendentals=0
        )
        return pl.pallas_call(
            body,
            in_specs=[vmem] * len(args) if specs is None else specs,
            out_specs=[vmem] * len(outs) if out_specs is None else out_specs,
            out_shape=outs,
            scratch_shapes=list(scratch),
            input_output_aliases=aliases,
            cost_estimate=estimate,
            compiler_params=pltpu.CompilerParams(vmem_limit_bytes=16 * 2**20),
        )(*args)

    rows_f32 = pltpu.VMEM((rows, feats), F32)
    rows_b16 = pltpu.VMEM((rows, feats), BF16)
    turn_f32 = pltpu.VMEM((feats, rows), F32)
    turn_b16 = pltpu.VMEM((feats, rows), BF16)
    wide_tab = pltpu.VMEM((heads, 4 * half), F32)
    table_shape = pltpu.VMEM((heads, table_len), F32)
    tile_shape = pltpu.VMEM((heads, 3, half, half), F32)
    stat_shape = pltpu.VMEM((2 * heads, rows), F32)
    line_shape = pltpu.VMEM((heads, rows), F32)
    out_shape = jax.ShapeDtypeStruct((rows, feats), BF16)
    body = functools.partial

    def at_hbm(array):
        return pltpu.with_memory_space_constraint(array, pltpu.HBM)

    def packed_shape(height, width):
        return pltpu.VMEM((height + pack_height(2 * heads, rows, width), width), BF16)

    query_far = shifted(query_rows, -2)
    query_in = shifted(query_rows, -1)
    far, first, second, stats = call(
        prep_kernel, 1,
        [packed_shape(rows, feats), packed_shape(rows, cut),
         pltpu.VMEM((rows, feats - cut), BF16), stat_shape],
        tuple(at_hbm(x) for x in (out_grad, log_totals.T, out_dot.T)),
        (line_shape, line_shape, pltpu.SemaphoreType.DMA((5,))),
        [hbm] * 3,
    )
    far_in = shifted(far, -2)
    first_in = shifted(first, -1)
    second_in = shifted(second, -1)

    dq0, dk, dv, tab, turned, tiles, chunks, keys, values = call(
        body(lag_kernel, 0, 0, heads, 2, heads), 5 * heads,
        [turn_f32, rows_f32, rows_f32, wide_tab, turn_b16, tile_shape, wide_tab,
         rows_b16, rows_b16],
        tuple(at_hbm(x) for x in (key_rows, value_rows, query_rows, bias_table))
        + (far, stats),
        (rows_b16, table_shape, pltpu.SemaphoreType.DMA((4,))),
        [hbm] * 4 + [vmem] * 2,
    )
    shared = (keys, values, turned, tiles, chunks)
    dk, dv, tab, dq2, _ = call(
        body(lag_kernel, 2, 0, heads, 2, heads), 5 * heads,
        [rows_f32, rows_f32, wide_tab, turn_b16, stat_shape],
        shared + (dk, dv, tab, query_far, far_in), aliases={5: 0, 6: 1, 7: 2},
    )
    back_far = shifted(dq2, 2)
    dk, dv, tab, dq1, stats_in = call(
        body(lag_kernel, 1, 0, cut_head, 2, heads), 5 * cut_head,
        [rows_f32, rows_f32, wide_tab, turn_b16, stat_shape],
        shared + (dk, dv, tab) + (query_in, first_in), aliases={5: 0, 6: 1, 7: 2},
    )
    dk, dv, table_part, dq1 = call(
        body(lag_kernel, 1, cut_head, heads, 2, heads), 5 * (heads - cut_head),
        [rows_f32, rows_f32, table_shape, turn_b16],
        shared + (dk, dv, tab) + (query_in, second_in, stats_in, dq1),
        aliases={5: 0, 6: 1, 11: 3},
    )
    back_near = shifted(dq1, 1)
    grad_table = all_sum(table_part)
    grad_query, grad_key, grad_value = call(
        body(close_kernel, 2, heads), 1, [out_shape] * 3,
        (dq0, back_near, back_far, dk, dv),
        (rows_b16,) * 3 + (pltpu.SemaphoreType.DMA((3,)),),
        out_specs=[hbm] * 3,
    )
    return grad_query, grad_key, grad_value, grad_table


def solution(mesh):
    placed = (P(AXES, None),) * 6 + (P(),)
    return jax.shard_map(
        local,
        mesh=mesh,
        in_specs=placed,
        out_specs=(P(AXES, None),) * 3 + (P(),),
        check_vma=False,
    )
```

time: 71.9 us -> 63.1 us (0.88)
  waiting for transfers between devices: 28.9 us -> 21.3 us
  starting transfers between devices: 21.3 us -> 25 us
  other arithmetic: 3.2 us -> 0.62 us
  local copies, waits for them, and re-layouts: 1.17 us -> 0 us
  Pallas kernels: 16.1 us -> 15 us
    ppermute x7, waiting for transfers between devices: 12 us -> 8.06 us  [all_sum(): lax.ppermute(part, AXES, [(i, i ^ mask) for i in range(count)])]
    ppermute x6 -> x7, waiting for transfers between devices: 17 us -> 13.2 us  [shifted(): return lax.ppermute(block, AXES, route)]
    ppermute x6 -> x7, starting transfers between devices: 12 us -> 15.2 us  [shifted(): return lax.ppermute(block, AXES, route)]
    concatenate x2 -> x0, other arithmetic: 1.1 us -> none  [the longest x1 1.09 us: packed_grads(): return jnp.concatenate([out_grad, terms], axis=1)]
    pallas_call x6, Pallas kernels: 16.1 us -> 15 us  [call(): pl.pallas_call(body, in_specs=[vmem] * len(args) if specs is None else sp...]
    unnamed x8 -> x0, local copies, waits for them, and re-layouts: 1.05 us -> none
    mul x1 -> x0, other arithmetic: 0.79 us -> none  [packed_grads(): stats = jnp.concatenate([log_totals * LOG2E, out_dot], axis=1)]
  transfers between devices with their start and end apart: 13 -> 14, of which waited for: 6 -> 7; matrix products, arithmetic and copies ran while one was open for 1% -> 1% of each run, Pallas kernels for 16% -> 18%
where the time goes in v4:
time: 63.1 us; the launch traced here: 62.6 us
  starting transfers between devices  25 us (40%)
  waiting for transfers between devices  21.3 us (34%)
  Pallas kernels  15 us (24%)
  between operations  0.74 us (1%)
    ppermute x7, starting transfers between devices, shifted(): return lax.ppermute(block, AXES, route)  15.2 us
    pallas_call x6, Pallas kernels, call(): pl.pallas_call(body, in_specs=[vmem] * len(args) if specs is None else sp...  15 us
    ppermute x7, waiting for transfers between devices, shifted(): return lax.ppermute(block, AXES, route)  13.2 us
    ppermute x7, starting transfers between devices, all_sum(): lax.ppermute(part, AXES, [(i, i ^ mask) for i in range(count)])  9.81 us
    ppermute x7, waiting for transfers between devices, all_sum(): lax.ppermute(part, AXES, [(i, i ^ mask) for i in range(count)])  8.06 us
  transfers between devices with their start and end apart: 14, of which 7 were waited for; matrix products, arithmetic and copies ran while one was open for 1% of the time, Pallas kernels for 18%

profile of v4, /device:TPU:0, one launch (start us, length us, event | category | flops | bytes accessed | tf_op | source)
XLA Modules:
  0.0 62.6 jit_solution(7457140756319056999)
XLA Ops:
  0.6 1.3 %shard_map.102 = (bf16[272,1024]{1,0:T(8,128)(2,1)S(1)}, bf16[272,768]{1,0:T(8,128)(2,1)S(1)}, bf16[256,256]{1,0:T(8,128)(2,1)S(1)}, f32[16,256]{1,0:T(8,128)S(1)}) custom-call(bf16[256,1024]{1,0:T(8,128)(2,1)} %g_hbm.1, f32[8,256]{1,0:T(8,128)} %bitcast.2, f32[8,256]{1,0:T(8,128)} %bitcast.3), custom_call_target="tpu_custom_call" | custom-call | flops 16777216 | bytes 2097152 | tf_op jit(solution)/shard_map/pallas_call | solution.py:384
  1.9 1.3 %collective-permute-start.1 = (bf16[272,1024]{1,0:T(8,128)(2,1)S(1)}, bf16[272,1024]{1,0:T(8,128)(2,1)S(1)}, u32[]{:S(2)}, u32[]{:S(2)}) collective-permute-start(bf16[272,1024]{1,0:T(8,128)(2,1)S(1)} %get-tuple-element.33.refs_4_), channel_id=1, source_target_pairs={{2,0},{3,1},{4,2},{5,3},{6,4},{7,5},{8,6},{9,7},{10,8},{11,9},{12,... | collective-permute-start | bytes 1671176 | tf_op jit(solution)/shard_map/ppermute | solution.py:27
  3.2 1.3 %collective-permute-start = (bf16[256,1024]{1,0:T(8,128)(2,1)}, bf16[256,1024]{1,0:T(8,128)(2,1)S(1)}, u32[]{:S(2)}, u32[]{:S(2)}) collective-permute-start(bf16[256,1024]{1,0:T(8,128)(2,1)} %refs_2_.1), channel_id=1, source_target_pairs={{2,0},{3,1},{4,2},{5,3},{6,4},{7,5},{8,6},{9,7},{10,8},{11,9},{12,... | collective-permute-start | bytes 1572872 | tf_op jit(solution)/shard_map/ppermute | solution.py:27
  4.5 1.3 %collective-permute-start.2 = (bf16[256,1024]{1,0:T(8,128)(2,1)}, bf16[256,1024]{1,0:T(8,128)(2,1)S(1)}, u32[]{:S(2)}, u32[]{:S(2)}) collective-permute-start(bf16[256,1024]{1,0:T(8,128)(2,1)} %refs_2_.1), channel_id=1, source_target_pairs={{1,0},{2,1},{3,2},{4,3},{5,4},{6,5},{7,6},{8,7},{9,8},{10,9},{11,1... | collective-permute-start | bytes 1572872 | tf_op jit(solution)/shard_map/ppermute | solution.py:27
  5.8 1.3 %collective-permute-start.3 = (bf16[272,768]{1,0:T(8,128)(2,1)S(1)}, bf16[272,768]{1,0:T(8,128)(2,1)S(1)}, u32[]{:S(2)}, u32[]{:S(2)}) collective-permute-start(bf16[272,768]{1,0:T(8,128)(2,1)S(1)} %get-tuple-element.47), channel_id=1, source_target_pairs={{1,0},{2,1},{3,2},{4,3},{5,4},{6,5},{7,6},{8,7},{9,8},{10,9},{11,1... | collective-permute-start | bytes 1253384 | tf_op jit(solution)/shard_map/ppermute | solution.py:27
  7.1 1.3 %collective-permute-start.4 = (bf16[256,256]{1,0:T(8,128)(2,1)S(1)}, bf16[256,256]{1,0:T(8,128)(2,1)S(1)}, u32[]{:S(2)}, u32[]{:S(2)}) collective-permute-start(bf16[256,256]{1,0:T(8,128)(2,1)S(1)} %get-tuple-element.51), channel_id=1, source_target_pairs={{1,0},{2,1},{3,2},{4,3},{5,4},{6,5},{7,6},{8,7},{9,8},{10,9},{11,1... | collective-permute-start | bytes 393224 | tf_op jit(solution)/shard_map/ppermute | solution.py:27
  8.4 5.3 %shard_map.103 = (f32[1024,256]{1,0:T(8,128)S(1)}, f32[256,1024]{1,0:T(8,128)S(1)}, f32[256,1024]{1,0:T(8,128)S(1)}, f32[8,512]{1,0:T(8,128)S(1)}, bf16[1024,256...) custom-call(bf16[256,1024]{1,0:T(8,128)(2,1)} %refs_0_.1, ...), custom_call_target="tpu_custom_call" | custom-call | flops 671088640 | bytes 2097152 | tf_op jit(solution)/shard_map/pallas_call | solution.py:384
  13.8 0.0 collective-permute-done.1.refs_9_
  13.8 3.5 %shard_map.104 = (f32[256,1024]{1,0:T(8,128)S(1)}, f32[256,1024]{1,0:T(8,128)S(1)}, f32[8,512]{1,0:T(8,128)S(1)}, bf16[1024,256]{1,0:T(8,128)(2,1)S(1)}, f32[16,256]{1,0:T(8,128)}) custom-call(bf16[256,1024]{1,0:T(8,128)(2,1)S(1)} %get-tuple-element.36.refs_0_, ...), custom_call_target="tpu_custom_call", output_to_operand_aliasing={{0}: (5, {}), {1}: (6, {}), {2}: (7, {})} | custom-call | flops 671088640 | bytes 2097152 | tf_op jit(solution)/shard_map/pallas_call | solution.py:384
  17.2 13.0 %collective-permute-done.3.refs_9_ = bf16[272,768]{1,0:T(8,128)(2,1)S(1)} collective-permute-done((bf16[272,768]{1,0:T(8,128)(2,1)S(1)}, bf16[272,768]{1,0:T(8,128)(2,1)S(1)}, u32[]{:S(2)}, u32[]{:S(2)}) %collective-permute-start.3) | collective-permute-done | bytes 417824 | tf_op jit(solution)/shard_map/ppermute | solution.py:27
  30.2 2.6 %shard_map.105 = (f32[256,1024]{1,0:T(8,128)S(1)}, f32[256,1024]{1,0:T(8,128)S(1)}, f32[8,512]{1,0:T(8,128)S(1)}, bf16[1024,256]{1,0:T(8,128)(2,1)S(1)}, f32[16,256]{1,0:T(8,128)S(1)}) custom-call(bf16[256,1024]{1,0:T(8,128)(2,1)S(1)} %get-tuple-element.36.refs_0_, ...), custom_call_target="tpu_custom_call", output_to_operand_aliasing={{0}: (5, {}), {1}: (6, {}), {2}: (7, {})} | custom-call | flops 503316480 | bytes 2097152 | tf_op jit(solution)/shard_map/pallas_call | solution.py:384
  32.8 0.2 collective-permute-done.4.refs_9_
  33.0 0.9 %shard_map.106 = (f32[256,1024]{1,0:T(8,128)S(1)}, f32[256,1024]{1,0:T(8,128)S(1)}, f32[8,320]{1,0:T(8,128)S(1)}, bf16[1024,256]{1,0:T(8,128)(2,1)S(1)}) custom-call(bf16[256,1024]{1,0:T(8,128)(2,1)S(1)} %get-tuple-element.36.refs_0_, bf16[256,1024]{1,0:T(8,128)(2,1)S(1)} %get-tuple-element.37.refs_1_, ...), custom_call_target="tpu_custom_call", output_to_operand_aliasing={{0}: (5, {}), {1}: (6, {}), {3}: (11, {})} | custom-call | flops 167772160 | bytes 2097152 | tf_op jit(solution)/shard_map/pallas_call | solution.py:384
  34.0 5.6 %collective-permute-start.5 = (bf16[1024,256]{1,0:T(8,128)(2,1)S(1)}, bf16[1024,256]{1,0:T(8,128)(2,1)S(1)}, u32[]{:S(2)}, u32[]{:S(2)}) collective-permute-start(bf16[1024,256]{1,0:T(8,128)(2,1)S(1)} %get-tuple-element.54), channel_id=1, source_target_pairs={{0,1},{1,2},{2,3},{3,4},{4,5},{5,6},{6,7},{7,8},{8,9},{9,10},{10,1... | collective-permute-start | bytes 1572872 | tf_op jit(solution)/shard_map/ppermute | solution.py:27
  39.6 3.1 %collective-permute-start.6 = (bf16[1024,256]{1,0:T(8,128)(2,1)S(1)}, bf16[1024,256]{1,0:T(8,128)(2,1)S(1)}, u32[]{:S(2)}, u32[]{:S(2)}) collective-permute-start(bf16[1024,256]{1,0:T(8,128)(2,1)S(1)} %get-tuple-element.55), channel_id=1, source_target_pairs={{0,2},{1,3},{2,4},{3,5},{4,6},{5,7},{6,8},{7,9},{8,10},{9,11},{10,... | collective-permute-start | bytes 1572872 | tf_op jit(solution)/shard_map/ppermute | solution.py:27
  42.7 1.1 %collective-permute-start.7 = (f32[8,320]{1,0:T(8,128)S(1)}, f32[8,320]{1,0:T(8,128)S(1)}, u32[]{:S(2)}, u32[]{:S(2)}) collective-permute-start(f32[8,320]{1,0:T(8,128)S(1)} %get-tuple-element.61), channel_id=1, source_target_pairs={{0,2},{1,3},{2,0},{3,1},{4,6},{5,7},{6,4},{7,5},{8,10},{9,11},{10,... | collective-permute-start | bytes 30728 | tf_op jit(solution)/shard_map/ppermute | solution.py:67
  43.8 0.8 %collective-permute-done.7 = f32[8,320]{1,0:T(8,128)S(1)} collective-permute-done((f32[8,320]{1,0:T(8,128)S(1)}, f32[8,320]{1,0:T(8,128)S(1)}, u32[]{:S(2)}, u32[]{:S(2)}) %collective-permute-start.7) | collective-permute-done | bytes 10272 | tf_op jit(solution)/shard_map/ppermute | solution.py:67
  44.7 3.7 %collective-permute-start.9 = (f32[8,320]{1,0:T(8,128)S(1)}, f32[8,320]{1,0:T(8,128)S(1)}, u32[]{:S(2)}, u32[]{:S(2)}) collective-permute-start(f32[8,320]{1,0:T(8,128)S(1)} %add.21), channel_id=1, source_target_pairs={{0,16},{1,17},{2,18},{3,19},{4,20},{5,21},{6,22},{7,23},{8,24},{9,... | collective-permute-start | bytes 30728 | tf_op jit(solution)/shard_map/ppermute | solution.py:67
  48.4 1.4 %collective-permute-start.10 = (f32[8,320]{1,0:T(8,128)S(1)}, f32[8,320]{1,0:T(8,128)S(1)}, u32[]{:S(2)}, u32[]{:S(2)}) collective-permute-start(f32[8,320]{1,0:T(8,128)S(1)} %add.21), channel_id=1, source_target_pairs={{0,24},{1,25},{2,26},{3,27},{4,28},{5,29},{6,30},{7,31},{8,16},{9,... | collective-permute-start | bytes 30728 | tf_op jit(solution)/shard_map/ppermute | solution.py:67
  49.7 0.0 collective-permute-start.8
  49.8 0.3 collective-permute-done.9
  50.1 3.8 %collective-permute-done.10 = f32[8,320]{1,0:T(8,128)S(1)} collective-permute-done((f32[8,320]{1,0:T(8,128)S(1)}, f32[8,320]{1,0:T(8,128)S(1)}, u32[]{:S(2)}, u32[]{:S(2)}) %collective-permute-start.10) | collective-permute-done | bytes 10272 | tf_op jit(solution)/shard_map/ppermute | solution.py:67
  53.9 0.0 collective-permute-done.8
  53.9 2.1 %collective-permute-start.12 = (f32[8,320]{1,0:T(8,128)S(1)}, f32[8,320]{1,0:T(8,128)S(1)}, u32[]{:S(2)}, u32[]{:S(2)}) collective-permute-start(f32[8,320]{1,0:T(8,128)S(1)} %add_add_fusion.1), channel_id=1, source_target_pairs={{0,4},{1,5},{2,6},{3,7},{4,0},{5,1},{6,2},{7,3},{8,12},{9,13},{10,... | collective-permute-start | bytes 30728 | tf_op jit(solution)/shard_map/ppermute | solution.py:67
  56.0 0.0 collective-permute-start.13
  56.0 1.5 %collective-permute-start.11 = (f32[8,320]{1,0:T(8,128)S(1)}, f32[8,320]{1,0:T(8,128)S(1)}, u32[]{:S(2)}, u32[]{:S(2)}) collective-permute-start(f32[8,320]{1,0:T(8,128)S(1)} %add_add_fusion.1), channel_id=1, source_target_pairs={{0,1},{1,0},{2,3},{3,2},{4,5},{5,4},{6,7},{7,6},{8,9},{9,8},{10,11... | collective-permute-start | bytes 30728 | tf_op jit(solution)/shard_map/ppermute | solution.py:67
  57.5 0.2 collective-permute-done.12
  57.7 2.9 %collective-permute-done.13 = f32[8,320]{1,0:T(8,128)S(1)} collective-permute-done((f32[8,320]{1,0:T(8,128)S(1)}, f32[8,320]{1,0:T(8,128)S(1)}, u32[]{:S(2)}, u32[]{:S(2)}) %collective-permute-start.13) | collective-permute-done | bytes 10272 | tf_op jit(solution)/shard_map/ppermute | solution.py:67
  60.6 0.0 collective-permute-done.11
  60.6 0.6 add_add_fusion
  61.2 0.0 collective-permute-done.5.one_ref
  61.2 1.4 %shard_map.107 = (bf16[256,1024]{1,0:T(8,128)(2,1)}, bf16[256,1024]{1,0:T(8,128)(2,1)}, bf16[256,1024]{1,0:T(8,128)(2,1)}) custom-call(f32[1024,256]{1,0:T(8,128)S(1)} %get-tuple-element.35.dq_ref, bf16[1024,256]{1,0:T(8,128)(2,1)S(1)} %collective-permute-done.5.one_ref, bf16[1024,256]{1,0:T(8,128)(2,1)S(1)} %collective-permute-done.6.two_ref, ...), custom_call_target="tpu_custom_call" | custom-call | flops 16777216 | bytes 2097152 | tf_op jit(solution)/shard_map/pallas_call | solution.py:384
  (5 shorter events, 0.0 us)
Async XLA Ops:
  1.9 11.9 %collective-permute-start.1 = (bf16[272,1024]{1,0:T(8,128)(2,1)S(1)}, bf16[272,1024]{1,0:T(8,128)(2,1)S(1)}, u32[]{:S(2)}, u32[]{:S(2)}) collective-permute-start(bf16[272,1024]{1,0:T(8,128)(2,1)S(1)} %get-tuple-element.33.refs_4_), channel_id=1, source_target_pairs={{2,0},{3,1},{4,2},{5,3},{6,4},{7,5},{8,6},{9,7},{10,8},{11,9},{12,... | collective-permute-start | bytes 1671176 | tf_op jit(solution)/shard_map/ppermute | solution.py:27
  3.2 10.6 %collective-permute-start = (bf16[256,1024]{1,0:T(8,128)(2,1)}, bf16[256,1024]{1,0:T(8,128)(2,1)S(1)}, u32[]{:S(2)}, u32[]{:S(2)}) collective-permute-start(bf16[256,1024]{1,0:T(8,128)(2,1)} %refs_2_.1), channel_id=1, source_target_pairs={{2,0},{3,1},{4,2},{5,3},{6,4},{7,5},{8,6},{9,7},{10,8},{11,9},{12,... | collective-permute-start | bytes 1572872 | tf_op jit(solution)/shard_map/ppermute | solution.py:27
  4.5 25.7 %collective-permute-start.2 = (bf16[256,1024]{1,0:T(8,128)(2,1)}, bf16[256,1024]{1,0:T(8,128)(2,1)S(1)}, u32[]{:S(2)}, u32[]{:S(2)}) collective-permute-start(bf16[256,1024]{1,0:T(8,128)(2,1)} %refs_2_.1), channel_id=1, source_target_pairs={{1,0},{2,1},{3,2},{4,3},{5,4},{6,5},{7,6},{8,7},{9,8},{10,9},{11,1... | collective-permute-start | bytes 1572872 | tf_op jit(solution)/shard_map/ppermute | solution.py:27
  5.8 24.4 %collective-permute-start.3 = (bf16[272,768]{1,0:T(8,128)(2,1)S(1)}, bf16[272,768]{1,0:T(8,128)(2,1)S(1)}, u32[]{:S(2)}, u32[]{:S(2)}) collective-permute-start(bf16[272,768]{1,0:T(8,128)(2,1)S(1)} %get-tuple-element.47), channel_id=1, source_target_pairs={{1,0},{2,1},{3,2},{4,3},{5,4},{6,5},{7,6},{8,7},{9,8},{10,9},{11,1... | collective-permute-start | bytes 1253384 | tf_op jit(solution)/shard_map/ppermute | solution.py:27
  7.1 26.0 %collective-permute-start.4 = (bf16[256,256]{1,0:T(8,128)(2,1)S(1)}, bf16[256,256]{1,0:T(8,128)(2,1)S(1)}, u32[]{:S(2)}, u32[]{:S(2)}) collective-permute-start(bf16[256,256]{1,0:T(8,128)(2,1)S(1)} %get-tuple-element.51), channel_id=1, source_target_pairs={{1,0},{2,1},{3,2},{4,3},{5,4},{6,5},{7,6},{8,7},{9,8},{10,9},{11,1... | collective-permute-start | bytes 393224 | tf_op jit(solution)/shard_map/ppermute | solution.py:27
  34.0 27.2 %collective-permute-start.5 = (bf16[1024,256]{1,0:T(8,128)(2,1)S(1)}, bf16[1024,256]{1,0:T(8,128)(2,1)S(1)}, u32[]{:S(2)}, u32[]{:S(2)}) collective-permute-start(bf16[1024,256]{1,0:T(8,128)(2,1)S(1)} %get-tuple-element.54), channel_id=1, source_target_pairs={{0,1},{1,2},{2,3},{3,4},{4,5},{5,6},{6,7},{7,8},{8,9},{9,10},{10,1... | collective-permute-start | bytes 1572872 | tf_op jit(solution)/shard_map/ppermute | solution.py:27
  39.6 21.6 %collective-permute-start.6 = (bf16[1024,256]{1,0:T(8,128)(2,1)S(1)}, bf16[1024,256]{1,0:T(8,128)(2,1)S(1)}, u32[]{:S(2)}, u32[]{:S(2)}) collective-permute-start(bf16[1024,256]{1,0:T(8,128)(2,1)S(1)} %get-tuple-element.55), channel_id=1, source_target_pairs={{0,2},{1,3},{2,4},{3,5},{4,6},{5,7},{6,8},{7,9},{8,10},{9,11},{10,... | collective-permute-start | bytes 1572872 | tf_op jit(solution)/shard_map/ppermute | solution.py:27
  42.7 2.0 %collective-permute-start.7 = (f32[8,320]{1,0:T(8,128)S(1)}, f32[8,320]{1,0:T(8,128)S(1)}, u32[]{:S(2)}, u32[]{:S(2)}) collective-permute-start(f32[8,320]{1,0:T(8,128)S(1)} %get-tuple-element.61), channel_id=1, source_target_pairs={{0,2},{1,3},{2,0},{3,1},{4,6},{5,7},{6,4},{7,5},{8,10},{9,11},{10,... | collective-permute-start | bytes 30728 | tf_op jit(solution)/shard_map/ppermute | solution.py:67
  44.7 5.4 %collective-permute-start.9 = (f32[8,320]{1,0:T(8,128)S(1)}, f32[8,320]{1,0:T(8,128)S(1)}, u32[]{:S(2)}, u32[]{:S(2)}) collective-permute-start(f32[8,320]{1,0:T(8,128)S(1)} %add.21), channel_id=1, source_target_pairs={{0,16},{1,17},{2,18},{3,19},{4,20},{5,21},{6,22},{7,23},{8,24},{9,... | collective-permute-start | bytes 30728 | tf_op jit(solution)/shard_map/ppermute | solution.py:67
  48.4 5.5 %collective-permute-start.10 = (f32[8,320]{1,0:T(8,128)S(1)}, f32[8,320]{1,0:T(8,128)S(1)}, u32[]{:S(2)}, u32[]{:S(2)}) collective-permute-start(f32[8,320]{1,0:T(8,128)S(1)} %add.21), channel_id=1, source_target_pairs={{0,24},{1,25},{2,26},{3,27},{4,28},{5,29},{6,30},{7,31},{8,16},{9,... | collective-permute-start | bytes 30728 | tf_op jit(solution)/shard_map/ppermute | solution.py:67
  49.7 4.1 %collective-permute-start.8 = (f32[8,320]{1,0:T(8,128)S(1)}, f32[8,320]{1,0:T(8,128)S(1)}, u32[]{:S(2)}, u32[]{:S(2)}) collective-permute-start(f32[8,320]{1,0:T(8,128)S(1)} %add.21), channel_id=1, source_target_pairs={{0,8},{1,9},{2,10},{3,11},{4,12},{5,13},{6,14},{7,15},{8,0},{9,1},... | collective-permute-start | bytes 30728 | tf_op jit(solution)/shard_map/ppermute | solution.py:67
  53.9 3.8 %collective-permute-start.12 = (f32[8,320]{1,0:T(8,128)S(1)}, f32[8,320]{1,0:T(8,128)S(1)}, u32[]{:S(2)}, u32[]{:S(2)}) collective-permute-start(f32[8,320]{1,0:T(8,128)S(1)} %add_add_fusion.1), channel_id=1, source_target_pairs={{0,4},{1,5},{2,6},{3,7},{4,0},{5,1},{6,2},{7,3},{8,12},{9,13},{10,... | collective-permute-start | bytes 30728 | tf_op jit(solution)/shard_map/ppermute | solution.py:67
  56.0 4.6 %collective-permute-start.13 = (f32[8,320]{1,0:T(8,128)S(1)}, f32[8,320]{1,0:T(8,128)S(1)}, u32[]{:S(2)}, u32[]{:S(2)}) collective-permute-start(f32[8,320]{1,0:T(8,128)S(1)} %add_add_fusion.1), channel_id=1, source_target_pairs={{0,5},{1,4},{2,7},{3,6},{4,1},{5,0},{6,3},{7,2},{8,13},{9,12},{10,... | collective-permute-start | bytes 30728 | tf_op jit(solution)/shard_map/ppermute | solution.py:67
  56.0 4.6 %collective-permute-start.11 = (f32[8,320]{1,0:T(8,128)S(1)}, f32[8,320]{1,0:T(8,128)S(1)}, u32[]{:S(2)}, u32[]{:S(2)}) collective-permute-start(f32[8,320]{1,0:T(8,128)S(1)} %add_add_fusion.1), channel_id=1, source_target_pairs={{0,1},{1,0},{2,3},{3,2},{4,5},{5,4},{6,7},{7,6},{8,9},{9,8},{10,11... | collective-permute-start | bytes 30728 | tf_op jit(solution)/shard_map/ppermute | solution.py:67
